TPU v7x, 256 devices: a 4x2x16 block of a 4x16x16 slice. The times are simulated.
256 devices in a mesh: grp: 2 (over y), sp: 32 (over z, core), tp: 4 (over x).
Axes of the slice: x: 4, y: 2, z: 16, core: 2. Of those that a mesh axis runs over, the one named last changes fastest.
The devices are a block of a 4x16x16 slice.
Arguments:
- queries_small: bfloat16 [16384, 1024], P(('grp', 'sp'), 'tp'), parts along dimension 0, may hold values from -6 to 6
- keys_small: bfloat16 [16384, 512], P(('grp', 'sp'), 'tp'), parts along dimension 0, may hold values from -6 to 6
- values_small: bfloat16 [16384, 512], P(('grp', 'sp'), 'tp'), parts along dimension 0, may hold values from -6 to 6
- queries_large: bfloat16 [16384, 1024], P(('grp', 'sp'), 'tp'), parts along dimension 0, may hold values from -6 to 6
- keys_large: bfloat16 [16384, 512], P(('grp', 'sp'), 'tp'), parts along dimension 0, may hold values from -6 to 6
- values_large: bfloat16 [16384, 512], P(('grp', 'sp'), 'tp'), parts along dimension 0, may hold values from -6 to 6
- query_gain_small: float32 [128], P('grp'), parts along dimension 0, may hold values from 1.2 to 12
- key_gain_small: float32 [128], P('grp'), parts along dimension 0, may hold values from 1.2 to 12
- query_gain_large: float32 [256], P('grp'), parts along dimension 0, may hold values from 1.2 to 12
- key_gain_large: float32 [256], P('grp'), parts along dimension 0, may hold values from 1.2 to 12
- residual_in: bfloat16 [16384, 2048], P(('grp', 'sp', 'tp')), parts along dimension 0, may hold values from -1.5 to 1.5
- out_weight_small: bfloat16 [1024, 2048], P('tp'), may hold values from -0.125 to 0.125
- out_weight_large: bfloat16 [1024, 2048], P('tp'), may hold values from -0.125 to 0.125
- norm_gain: float32 [2048], replicated, may hold values from 0.1 to 1.9
- routes: int32 [16384, 2], P(('grp', 'sp', 'tp')), parts along dimension 0, may hold values from 0 to 63, all different within a row; in each aligned block of 64 rows (0 to 63, 64 to 127, ...) at most 4 rows name the same one
- route_scores: float32 [16384, 2], P(('grp', 'sp', 'tp')), parts along dimension 0, may hold values from 0.05 to 1
- expert_gate: bfloat16 [64, 2048, 1024], P('sp', None, 'tp'), may hold values from -0.125 to 0.125
- expert_up: bfloat16 [64, 2048, 1024], P('sp', None, 'tp'), may hold values from -0.125 to 0.125
- expert_down: bfloat16 [64, 1024, 2048], P('sp', 'tp'), may hold values from -0.1875 to 0.1875
Outputs:
- result: bfloat16 [16384, 2048], P(('grp', 'sp', 'tp')), parts along dimension 0
There are 2 independent parts, one for each index of `grp`. A program takes and returns all parts, laid end to end along the dimension named above; an argument that names none is the same for every part. Nothing has to cross between parts.
Inputs may be any that keep to these rules, and one draw needn't show every extreme that they name: `routes`: each token names 2 different experts; within the rows of one device (aligned blocks of 64 tokens) no expert is named more than 4 times, a bound that some block reaches.
All inputs are finite; a program needn't handle non-finite values.
Results may differ from a plain program's by a relative error of at most 0.02.
The roundings to bfloat16 on the way count: a program that leaves them out, or rounds other values in their place, can miss the bound.
Values may be sent and summed in bfloat16 or wider, within the bound.
A program may use at most 128 MiB of HBM per device.

v0:
```python
import jax
import jax.numpy as jnp
from jax import lax
from jax.sharding import PartitionSpec as P

HS_SMALL = 64
HS_LARGE = 128
GRID_W = 64


theta_base = 10000.0
norm_eps = 1e-06
block_target = 1280


def sent_together(arrays, axis, dim, along):
    ends, at = ([], 0)
    for a in arrays[:-1]:
        at += a.shape[along]
        ends.append(at)
    both = jnp.concatenate(arrays, axis=along)
    return tuple(jnp.split(lax.all_gather(both, axis, axis=dim, tiled=True), ends, axis=along))


def in_blocks(shard, dim, size):
    before, after = (shard.shape[:dim], shard.shape[dim + 1 :])
    return jnp.moveaxis(shard.reshape(*before, size, -1, *after), dim, 0)


def sent_and_summed(shard, axis, dim):
    blocks = in_blocks(shard, dim, lax.axis_size(axis))
    arrived = lax.all_to_all(blocks, axis, split_axis=0, concat_axis=0, tiled=True)
    return arrived.astype(jnp.float32).sum(axis=0)


def grid_tables(offset, length, head_size):
    places = offset + jnp.arange(length, dtype=jnp.int32)
    grid_rows = (places // GRID_W).astype(jnp.float32)
    grid_cols = (places % GRID_W).astype(jnp.float32)
    rates = jnp.power(
        theta_base, -2.0 * jnp.arange(head_size // 4, dtype=jnp.float32) / (head_size // 2)
    )
    row_angles = grid_rows[:, None, None] * rates
    col_angles = grid_cols[:, None, None] * rates
    return (jnp.cos(row_angles), jnp.sin(row_angles), jnp.cos(col_angles), jnp.sin(col_angles))


def half_turn(segment, cosine, sine_part):
    half_size = segment.shape[-1] // 2
    leading = segment[..., :half_size]
    trailing = segment[..., half_size:]
    return jnp.concatenate(
        [leading * cosine - trailing * sine_part, trailing * cosine + leading * sine_part], axis=-1
    )


def grid_turn(vectors, tables):
    row_cos, row_sin, col_cos, col_sin = tables
    half_size = vectors.shape[-1] // 2
    return jnp.concatenate(
        [
            half_turn(vectors[..., :half_size], row_cos, row_sin),
            half_turn(vectors[..., half_size:], col_cos, col_sin),
        ],
        axis=-1,
    )


def normed_turn(raw_rows, gain, tables):
    widened = raw_rows.astype(jnp.float32)
    scaled = (
        widened * lax.rsqrt(jnp.mean(widened * widened, axis=-1, keepdims=True) + norm_eps) * gain
    )
    return grid_turn(scaled, tables).astype(jnp.bfloat16)


def block_rows(row_count, shard_rows):
    shards = row_count // shard_rows
    chosen = 1
    for factor in range(1, max(1, block_target // shard_rows) + 1):
        if shards % factor == 0:
            chosen = factor
    return chosen * shard_rows


def attend_block(state, queries, key_rows, value_rows):
    largest, weight_sum, accumulated = state
    head_size = queries.shape[-1]
    kv_local = queries.shape[1]
    key_heads = key_rows.reshape(key_rows.shape[0], kv_local, head_size)
    value_heads = value_rows.reshape(value_rows.shape[0], kv_local, head_size)
    scores = jnp.einsum(
        "qgrd,kgd->qgrk", queries, key_heads, preferred_element_type=jnp.float32
    ) * head_size ** (-0.5)
    peak_score = jnp.maximum(largest, jnp.max(scores, axis=-1))
    shrink = jnp.exp(largest - peak_score)
    weights = jnp.exp(scores - peak_score[..., None])
    weight_sum = weight_sum * shrink + jnp.sum(weights, axis=-1)
    accumulated = accumulated * shrink[..., None] + jnp.einsum(
        "qgrk,kgd->qgrd",
        weights.astype(jnp.bfloat16),
        value_heads,
        preferred_element_type=jnp.float32,
    )
    return (peak_score, weight_sum, accumulated)


def attend_rows(state, queries, key_rows, value_rows):
    row_count = key_rows.shape[0]
    step_rows = block_rows(row_count, queries.shape[0])

    def one_block(block_index, carried):
        offset = block_index * step_rows
        return attend_block(
            carried,
            queries,
            lax.dynamic_slice_in_dim(key_rows, offset, step_rows, 0),
            lax.dynamic_slice_in_dim(value_rows, offset, step_rows, 0),
        )

    return lax.fori_loop(0, row_count // step_rows, one_block, state)


def empty_state(queries):
    state_shape = queries.shape[:3]
    return (
        jnp.full(state_shape, -1e30, jnp.float32),
        jnp.zeros(state_shape, jnp.float32),
        jnp.zeros(queries.shape, jnp.float32),
    )


def finish(state):
    largest, weight_sum, accumulated = state
    merged = accumulated / weight_sum[..., None]
    return merged.reshape(merged.shape[0], -1).astype(jnp.bfloat16)


def on_device(
    queries_small,
    keys_small,
    values_small,
    queries_large,
    keys_large,
    values_large,
    query_gain_small,
    key_gain_small,
    query_gain_large,
    key_gain_large,
    residual_in,
    out_weight_small,
    out_weight_large,
    norm_gain,
    routes,
    route_scores,
    expert_gate,
    expert_up,
    expert_down,
):
    token_rows = queries_small.shape[0]
    offset = lax.axis_index("sp") * token_rows
    tables_small = grid_tables(offset, token_rows, HS_SMALL)
    tables_large = grid_tables(offset, token_rows, HS_LARGE)
    kv_small = keys_small.shape[1] // HS_SMALL
    kv_large = keys_large.shape[1] // HS_LARGE
    asked_small = normed_turn(
        queries_small.reshape(token_rows, -1, HS_SMALL), query_gain_small, tables_small
    ).reshape(token_rows, kv_small, -1, HS_SMALL)
    asked_large = normed_turn(
        queries_large.reshape(token_rows, -1, HS_LARGE), query_gain_large, tables_large
    ).reshape(token_rows, kv_large, -1, HS_LARGE)
    turned_small = normed_turn(
        keys_small.reshape(token_rows, kv_small, HS_SMALL), key_gain_small, tables_small
    ).reshape(token_rows, -1)
    turned_large = normed_turn(
        keys_large.reshape(token_rows, kv_large, HS_LARGE), key_gain_large, tables_large
    ).reshape(token_rows, -1)
    key_small, value_small, key_large, value_large = sent_together(
        (turned_small, values_small, turned_large, values_large), "sp", 0, 1
    )
    state_small = attend_rows(empty_state(asked_small), asked_small, key_small, value_small)
    state_large = attend_rows(empty_state(asked_large), asked_large, key_large, value_large)
    heard_small = finish(state_small)
    heard_large = finish(state_large)
    projected = sent_and_summed(
        (
            jnp.dot(heard_small, out_weight_small, preferred_element_type=jnp.float32)
            + jnp.dot(heard_large, out_weight_large, preferred_element_type=jnp.float32)
        ).astype(jnp.bfloat16),
        "tp",
        0,
    )
    attended = (residual_in.astype(jnp.float32) + projected).astype(jnp.bfloat16)
    widened = attended.astype(jnp.float32)
    normed = (
        widened
        * lax.rsqrt(jnp.mean(widened * widened, axis=-1, keepdims=True) + norm_eps)
        * norm_gain
    ).astype(jnp.bfloat16)
    local_rows = routes.shape[0]
    top_count = routes.shape[1]
    sp_count = lax.axis_size("sp")
    local_experts = expert_gate.shape[0]
    expert_count = local_experts * sp_count
    capacity = max(2, (2 * top_count * local_rows + expert_count - 1) // expert_count)
    flat_routes = routes.reshape(-1)
    member = (flat_routes[:, None] == jnp.arange(expert_count, dtype=jnp.int32)[None, :]).astype(
        jnp.int32
    )
    ranks = jnp.sum((jnp.cumsum(member, axis=0) - member) * member, axis=1)
    slots = flat_routes * capacity + ranks
    picker = (
        slots[:, None] == jnp.arange(expert_count * capacity, dtype=jnp.int32)[None, :]
    ).astype(jnp.bfloat16)
    placer = jnp.sum(picker.reshape(local_rows, top_count, -1), axis=1)
    outgoing = jnp.einsum("ts,td->sd", placer, normed, preferred_element_type=jnp.float32).astype(
        jnp.bfloat16
    )
    outgoing = outgoing.reshape(sp_count, local_experts, capacity, -1)
    everyone = lax.all_gather(
        lax.all_to_all(outgoing, "sp", split_axis=0, concat_axis=0, tiled=True),
        "tp",
        axis=0,
        tiled=True,
    )
    gate_out = jnp.einsum(
        "secd,edf->secf", everyone, expert_gate, preferred_element_type=jnp.float32
    )
    up_out = jnp.einsum("secd,edf->secf", everyone, expert_up, preferred_element_type=jnp.float32)
    active = (jax.nn.silu(gate_out) * up_out).astype(jnp.bfloat16)
    summed = lax.psum_scatter(
        jnp.einsum(
            "secf,efd->secd", active, expert_down, preferred_element_type=jnp.float32
        ).astype(jnp.bfloat16),
        "tp",
        scatter_dimension=0,
        tiled=True,
    )
    returned = lax.all_to_all(summed, "sp", split_axis=0, concat_axis=0, tiled=True)
    back_rows = returned.reshape(expert_count * capacity, -1)
    chosen_rows = jnp.dot(picker, back_rows, preferred_element_type=jnp.float32).reshape(
        local_rows, top_count, -1
    )
    shares = route_scores / jnp.sum(route_scores, axis=1, keepdims=True)
    mixed = jnp.sum(chosen_rows * shares[:, :, None], axis=1)
    return (attended.astype(jnp.float32) + mixed).astype(jnp.bfloat16)


def solution(mesh):
    in_specs = (
        P(("grp", "sp"), "tp"),
        P(("grp", "sp"), "tp"),
        P(("grp", "sp"), "tp"),
        P(("grp", "sp"), "tp"),
        P(("grp", "sp"), "tp"),
        P(("grp", "sp"), "tp"),
        P("grp"),
        P("grp"),
        P("grp"),
        P("grp"),
        P(("grp", "sp", "tp"), None),
        P("tp", None),
        P("tp", None),
        P(),
        P(("grp", "sp", "tp"), None),
        P(("grp", "sp", "tp"), None),
        P("sp", None, "tp"),
        P("sp", None, "tp"),
        P("sp", "tp", None),
    )
    out_specs = P(("grp", "sp", "tp"), None)
    return jax.shard_map(
        on_device, mesh=mesh, in_specs=in_specs, out_specs=out_specs, check_vma=False
    )
```

profile of v0, /device:TPU:33, one launch (start us, length us, event | category | flops | bytes accessed | tf_op | source)
XLA Modules:
  0.0 520.4 jit_solution(17485946820454856762)
XLA Ops:
  15.2 107.8 %all-gather.3.cloned.1.call-done = bf16[8192,512]{0,1:T(8,128)(2,1)} async-done(((bf16[256,512]{0,1:T(8,128)(2,1)}), bf16[8192,512]{0,1:T(8,128)(2,1)}) %all-gather.3.cloned.1.call-update) | async-done | bytes 8388624 | tf_op jit(solution)/shard_map/all_gather | solution.py:22
  123.0 6.0 %fusion.100 = (bf16[8192,128]{0,1:T(8,128)(2,1)}, bf16[8192,128]{0,1:T(8,128)(2,1)}, bf16[8192,128]{0,1:T(8,128)(2,1)}, bf16[8192,128]{0,1:T(8,128)(2,1)}) fusion(bf16[8192,512]{0,1:T(8,128)(2,1)} %all-gather.3.cloned.1.call-done), kind=kLoop, calls=%fused_computation.172 | loop fusion | bytes 16777216 | tf_op jit(solution)/shard_map/split | solution.py:22
  129.0 44.6 %while.37 = (s32[]{:T(128)}, f32[256,1,2]{0,2,1:T(2,128)S(1)}, f32[256,1,2]{0,2,1:T(2,128)S(1)}, f32[256,1,2,128]{0,3,2,1:T(8,128)S(1)}, bf16[8192,128]{0,1:T(8,...) while((s32[]{:T(128)}, f32[256,1,2]{0,2,1:T(2,128)S(1)}, ...), condition=%wide.region_11.12_spmd.clone, body=%wide.region_8.11_spmd.clone.sunk | while | flops 272829440 | bytes 15892683 | solution.py:121
  129.0 2.8 bitcast_reduce_fusion.5
  131.8 2.4 fusion.138
  134.6 2.8 bitcast_reduce_fusion.5
  137.3 2.4 fusion.138
  140.1 2.8 bitcast_reduce_fusion.5
  142.9 2.4 fusion.138
  145.7 2.8 bitcast_reduce_fusion.5
  148.5 2.4 fusion.138
  151.3 2.8 bitcast_reduce_fusion.5
  154.1 2.4 fusion.138
  156.9 2.8 bitcast_reduce_fusion.5
  159.6 2.4 fusion.138
  162.4 2.8 bitcast_reduce_fusion.5
  165.2 2.4 fusion.138
  168.0 2.8 bitcast_reduce_fusion.5
  170.8 2.4 fusion.138
  173.6 64.9 %while.36 = (s32[]{:T(128)}, f32[256,2,2]{0,2,1:T(2,128)S(1)}, f32[256,2,2]{0,2,1:T(2,128)S(1)}, f32[256,2,2,64]{0,3,2,1:T(8,128)S(1)}, bf16[8192,128]{0,1:T(8,1...) while((s32[]{:T(128)}, f32[256,2,2]{0,2,1:T(2,128)S(1)}, ...), condition=%wide.region_6.7_spmd.clone, body=%wide.region_3.6_spmd.clone.sunk | while | flops 277025792 | bytes 31654084 | solution.py:121
  174.7 2.7 bitcast_reduce_fusion.4
  177.4 3.0 fusion.131
  182.8 2.7 bitcast_reduce_fusion.4
  185.5 3.0 fusion.131
  190.9 2.7 bitcast_reduce_fusion.4
  193.6 3.0 fusion.131
  199.0 2.7 bitcast_reduce_fusion.4
  201.7 3.0 fusion.131
  207.1 2.7 bitcast_reduce_fusion.4
  209.8 3.0 fusion.131
  215.2 2.7 bitcast_reduce_fusion.4
  217.9 3.0 fusion.131
  223.3 2.7 bitcast_reduce_fusion.4
  226.0 3.0 fusion.131
  231.5 2.7 bitcast_reduce_fusion.4
  234.1 3.0 fusion.131
  238.6 1.8 fusion.101
  241.8 4.1 all-to-all-start
  246.9 13.6 %all-to-all-done = bf16[4,64,2048]{2,1,0:T(8,128)(2,1)S(1)} async-done(((bf16[4,64,2048]{2,1,0:T(8,128)(2,1)}), bf16[4,64,2048]{2,1,0:T(8,128)(2,1)S(1)}, u32[]{:S(2)}, u32[]{:S(2)}) %all-to-all-start) | async-done | bytes 1048608 | tf_op jit(solution)/shard_map/all_to_all | solution.py:32
  263.6 64.4 %all_to_all.15 = bf16[32,2,4,2048]{3,2,1,0:T(4,128)(2,1)S(1)} all-to-all(bf16[32,2,4,2048]{3,2,1,0:T(4,128)(2,1)} %reshape.651), channel_id=1, replica_groups=mesh['grp'=2,'sp'=32,'tp'=4] {'sp'}, dimensions={0} | all-to-all | bytes 2097152 | tf_op jit(solution)/shard_map/all_to_all | solution.py:221
  329.9 43.8 %all-gather.5.cloned.1.call-done = bf16[128,2,4,2048]{3,0,2,1:T(8,128)(2,1)} async-done(((bf16[32,2,4,2048]{3,0,2,1:T(8,128)(2,1)}), bf16[128,2,4,2048]{3,0,2,1:T(8,128)(2,1)}) %all-gather.5.cloned.1.call-update) | async-done | bytes 4194320 | tf_op jit(solution)/shard_map/all_gather | solution.py:220
  373.7 4.1 fusion.38
  377.8 7.3 %convert_bitcast_fusion = bf16[128,2,4,2048]{3,0,2,1:T(8,128)(2,1)} fusion(bf16[2,256,2048]{2,1,0:T(8,128)(2,1)S(1)} %copy-done, bf16[128,2,4,2048]{3,0,2,1:T(8,128)(2,1)} %all-gather.5.cloned.1.call-done, bf16[2,2048,256]{2,1,0:T(8,128)(2,1)} %param.40, f32[128,2,4,256]{3,0,2,1:T(8,128)S(1)} %fusion.38), kind=kOutput, calls=%fused_computation.43 | convolution fusion | flops 2151153664 | bytes 13631488 | tf_op jit(solution)/shard_map/secf,efd->secd/dot_general | solution.py:232
  385.2 53.5 %reduce-scatter.2.cloned.1.call-done = bf16[32,2,4,2048]{3,0,2,1:T(8,128)(2,1)} async-done(((bf16[128,2,4,2048]{3,0,2,1:T(8,128)(2,1)}), bf16[32,2,4,2048]{3,0,2,1:T(8,128)(2,1)}) %reduce-scatter.2.cloned.1.call-update) | async-done | bytes 1048592 | tf_op jit(solution)/shard_map/reduce_scatter | solution.py:231
  438.7 3.1 copy.95
  441.8 13.2 %all-to-all-start.2 = ((bf16[32,2,4,2048]{3,2,1,0:T(4,128)(2,1)}), bf16[32,2,4,2048]{3,2,1,0:T(4,128)(2,1)S(1)}, u32[]{:S(2)}, u32[]{:S(2)}) async-start(bf16[32,2,4,2048]{3,2,1,0:T(4,128)(2,1)} %copy.95), calls=%async_computation.3 | async-start | bytes 2097152 | tf_op jit(solution)/shard_map/all_to_all | solution.py:239
  455.0 55.4 %all-to-all-done.2 = bf16[32,2,4,2048]{3,2,1,0:T(4,128)(2,1)S(1)} async-done(((bf16[32,2,4,2048]{3,2,1,0:T(4,128)(2,1)}), bf16[32,2,4,2048]{3,2,1,0:T(4,128)(2,1)S(1)}, u32[]{:S(2)}, u32[]{:S(2)}) %all-to-all-start.2) | async-done | bytes 1048608 | tf_op jit(solution)/shard_map/all_to_all | solution.py:239
  511.5 1.6 fusion.50
  (195 shorter events, 39.6 us)
Async XLA Ops:
  6.5 371.2 %copy-start = (bf16[2,256,2048]{2,1,0:T(8,128)(2,1)S(1)}, bf16[2,256,2048]{2,1,0:T(8,128)(2,1)}, u32[]{:S(2)}) copy-start(bf16[2,256,2048]{2,1,0:T(8,128)(2,1)} %param.41) | copy-start | bytes 6291460
  6.6 7.5 %copy-start.5 = (bf16[256,256]{1,0:T(8,128)(2,1)S(1)}, bf16[256,256]{1,0:T(8,128)(2,1)}, u32[]{:S(2)}) copy-start(bf16[256,256]{1,0:T(8,128)(2,1)} %param.26) | copy-start | bytes 393220
  6.6 8.0 %copy-start.10 = (f32[128]{0:T(128)S(1)}, f32[128]{0:T(128)}, u32[]{:S(2)}) copy-start(f32[128]{0:T(128)} %param.31) | copy-start | bytes 1540
  6.6 116.5 %all-gather.3.cloned.1.call-start = ((), (), s32[]{:S(2)}) async-start(), calls=%async_computation.4 | async-start | bytes 8650752 | tf_op jit(solution)/shard_map/all_gather | solution.py:22
  8.5 6.4 %copy-start.6 = (bf16[256,256]{1,0:T(8,128)(2,1)S(1)}, bf16[256,256]{1,0:T(8,128)(2,1)}, u32[]{:S(2)}) copy-start(bf16[256,256]{1,0:T(8,128)(2,1)} %param.23) | copy-start | bytes 393220
  8.7 6.3 %copy-start.11 = (f32[64]{0:T(128)S(1)}, f32[64]{0:T(128)}, u32[]{:S(2)}) copy-start(f32[64]{0:T(128)} %param.29) | copy-start | bytes 772
  13.2 0.7 copy-start.4
  131.7 2.4 copy-start.2
  137.3 2.4 copy-start.2
  142.9 2.4 copy-start.2
  148.5 2.4 copy-start.2
  154.1 2.4 copy-start.2
  159.6 2.4 copy-start.2
  165.2 2.4 copy-start.2
  170.8 2.4 copy-start.2
  177.4 3.4 copy-start.1
  185.5 3.4 copy-start.1
  193.6 3.4 copy-start.1
  201.7 3.4 copy-start.1
  209.8 3.4 copy-start.1
  217.9 3.4 copy-start.1
  226.0 3.4 copy-start.1
  234.1 3.4 copy-start.1
  238.5 1.8 copy-start.3
  241.8 4.1 copy-start.8
  241.8 20.1 %copy-start.7 = (f32[2048]{0:T(1024)S(1)}, f32[2048]{0:T(1024)}, u32[]{:S(2)}) copy-start(f32[2048]{0:T(1024)} %param.36) | copy-start | bytes 24580
  241.8 18.8 %all-to-all-start = ((bf16[4,64,2048]{2,1,0:T(8,128)(2,1)}), bf16[4,64,2048]{2,1,0:T(8,128)(2,1)S(1)}, u32[]{:S(2)}, u32[]{:S(2)}) async-start(bf16[4,64,2048]{2,1,0:T(8,128)(2,1)} %bitcast.205), calls=%async_computation | async-start | bytes 2097152 | tf_op jit(solution)/shard_map/all_to_all | solution.py:32
  245.9 127.8 %all-gather.5.cloned.1.call-start = ((), (), s32[]{:S(2)}) async-start(), calls=%async_computation.5 | async-start | bytes 5242880 | tf_op jit(solution)/shard_map/all_gather | solution.py:220
  329.6 109.1 %reduce-scatter.2.cloned.1.call-start = ((), (), s32[]{:S(2)}) async-start(), calls=%async_computation.6 | async-start | bytes 5242880 | tf_op jit(solution)/shard_map/reduce_scatter | solution.py:231
  385.2 69.8 %copy-start.9 = (f32[64,2]{0,1:T(2,128)S(1)}, f32[64,2]{0,1:T(2,128)}, u32[]{:S(2)}) copy-start(f32[64,2]{0,1:T(2,128)} %param.38) | copy-start | bytes 1540
  441.8 68.6 %all-to-all-start.2 = ((bf16[32,2,4,2048]{3,2,1,0:T(4,128)(2,1)}), bf16[32,2,4,2048]{3,2,1,0:T(4,128)(2,1)S(1)}, u32[]{:S(2)}, u32[]{:S(2)}) async-start(bf16[32,2,4,2048]{3,2,1,0:T(4,128)(2,1)} %copy.95), calls=%async_computation.3 | async-start | bytes 2097152 | tf_op jit(solution)/shard_map/all_to_all | solution.py:239
Sparse Core Ops, SparseCore 0:
  14.1 108.8 all-gather.2
  329.7 43.8 all-gather.4
  385.3 53.3 reduce-scatter.1
where the time goes:
time: 522 us; the launch traced here: 520 us
  waiting for transfers between devices  274 us (52%)
  matrix products  86.1 us (16%)
  blocking collectives  64.4 us (12%)
  other arithmetic  33.7 us (6%)
  local copies, waits for them, and re-layouts  30 us (6%)
  starting transfers between devices  17.5 us (3%)
  between operations  13.6 us (3%)
    all_gather x1, waiting for transfers between devices, sent_together(): lax.all_gather(both, axis, axis=dim, tiled=True)  108 us
    all_to_all x1, blocking collectives, on_device(): lax.all_to_all(outgoing, 'sp', split_axis=0, concat_axis=0, tiled=True)  64.4 us
    all_to_all x1, waiting for transfers between devices, on_device(): lax.all_to_all(summed, 'sp', split_axis=0, concat_axis=0, tiled=True)  55.4 us
    reduce_scatter x1, waiting for transfers between devices, on_device(): lax.psum_scatter(jnp.einsum('secf,efd->secd', active, expert_down, prefer...  53.5 us
    all_gather x1, waiting for transfers between devices, on_device(): lax.all_gather(lax.all_to_all(outgoing, 'sp', split_axis=0, concat_axis=0...  43.8 us
    dot_general x16, matrix products, attend_block(): jnp.einsum('qgrd,kgd->qgrk', queries, key_heads, preferred_element_type=j...  43.6 us
    reduce_sum x16, other arithmetic, attend_block(): weight_sum = weight_sum * shrink + jnp.sum(weights, axis=-1)  27.2 us
    dot_general x16, matrix products, attend_block(): jnp.einsum('qgrk,kgd->qgrd', weights.astype(jnp.bfloat16), value_heads, p...  25.8 us
  transfers between devices with their start and end apart: 5, of which 5 were waited for; matrix products, arithmetic and copies ran while one was open for 0% of the time, Pallas kernels for 0%

commit v1 on v0

--- a/solution.py
+++ b/solution.py
@@ -1,36 +1,334 @@
+import functools
 import jax
 import jax.numpy as jnp
 from jax import lax
+from jax.experimental import pallas as pl
+from jax.experimental.pallas import tpu as pltpu
 from jax.sharding import PartitionSpec as P
 
 HS_SMALL = 64
 HS_LARGE = 128
 GRID_W = 64
-
-
+LOG2E = 1.4426950408889634
 theta_base = 10000.0
 norm_eps = 1e-06
-block_target = 1280
-
-
-def sent_together(arrays, axis, dim, along):
-    ends, at = ([], 0)
-    for a in arrays[:-1]:
-        at += a.shape[along]
-        ends.append(at)
-    both = jnp.concatenate(arrays, axis=along)
-    return tuple(jnp.split(lax.all_gather(both, axis, axis=dim, tiled=True), ends, axis=along))
-
-
-def in_blocks(shard, dim, size):
-    before, after = (shard.shape[:dim], shard.shape[dim + 1 :])
-    return jnp.moveaxis(shard.reshape(*before, size, -1, *after), dim, 0)
-
-
-def sent_and_summed(shard, axis, dim):
-    blocks = in_blocks(shard, dim, lax.axis_size(axis))
-    arrived = lax.all_to_all(blocks, axis, split_axis=0, concat_axis=0, tiled=True)
-    return arrived.astype(jnp.float32).sum(axis=0)
+
+
+def _send(src, dst, ssem, rsem, axis, dev):
+    return pltpu.make_async_remote_copy(
+        src_ref=src,
+        dst_ref=dst,
+        send_sem=ssem,
+        recv_sem=rsem,
+        device_id={axis: dev},
+        device_id_type=pl.DeviceIdType.MESH,
+    )
+
+
+def attend_kernel(
+    heads,
+    kv_hbm,
+    qt_ref,
+    ws_hbm,
+    wl_hbm,
+    res_ref,
+    gain_ref,
+    att_ref,
+    nrm_ref,
+    rts_ref,
+    kvbuf,
+    wbuf,
+    acc,
+    mbuf,
+    lbuf,
+    hbuf,
+    pbuf,
+    xbuf,
+    lsem,
+    rsem,
+    ssem,
+    psem,
+    xr,
+    xs,
+):
+    n_sp = lax.axis_size("sp")
+    n_z = n_sp // 2
+    last = n_z // 2
+    tok = kvbuf.shape[3]
+    kv_rows = kvbuf.shape[2]
+    sp = lax.axis_index("sp")
+    tp = lax.axis_index("tp")
+    right = lax.rem(sp + 2, n_sp)
+    left = lax.rem(sp + n_sp - 2, n_sp)
+    partner = sp + 1 - 2 * lax.rem(sp, 2)
+    x_right = lax.rem(tp + 1, 4)
+    x_left = lax.rem(tp + 3, 4)
+    x_far = lax.rem(tp + 2, 4)
+
+    own = pltpu.make_async_copy(kv_hbm, kvbuf.at[0, 0], lsem.at[0])
+    own.start()
+    w_copies = [
+        pltpu.make_async_copy(ws_hbm, wbuf.at[pl.ds(0, 256)], lsem.at[1]),
+        pltpu.make_async_copy(wl_hbm, wbuf.at[pl.ds(256, 256)], lsem.at[2]),
+    ]
+    for w in w_copies:
+        w.start()
+
+    barrier = pltpu.get_barrier_semaphore()
+    for dev in (right, left, partner):
+        pl.semaphore_signal(
+            barrier, inc=1, device_id={"sp": dev}, device_id_type=pl.DeviceIdType.MESH
+        )
+    for dev in (x_right, x_left):
+        pl.semaphore_signal(
+            barrier, inc=1, device_id={"tp": dev}, device_id_type=pl.DeviceIdType.MESH
+        )
+    pl.semaphore_wait(barrier, 5)
+
+    parts = (pl.ds(0, tok), pl.ds(tok, kv_rows - tok))
+
+    def at(pair, side, part):
+        return kvbuf.at[pair, side, parts[part]]
+
+    def to_right(step, pair, part, dst_pair):
+        return _send(
+            at(pair, 0, part),
+            at(dst_pair, 0, part),
+            ssem.at[step, 0, part],
+            rsem.at[dst_pair, 0, part],
+            "sp",
+            right,
+        )
+
+    def to_left(step, pair, part, dst_pair, src_side=1, dst_side=1):
+        return _send(
+            at(pair, src_side, part),
+            at(dst_pair, dst_side, part),
+            ssem.at[step, 1, part],
+            rsem.at[dst_pair, dst_side, part],
+            "sp",
+            left,
+        )
+
+    def to_partner(pair, side, part, dst_pair, dst_side):
+        return _send(
+            at(pair, side, part),
+            at(dst_pair, dst_side, part),
+            psem.at[dst_pair, dst_side, part],
+            rsem.at[dst_pair, dst_side, part],
+            "sp",
+            partner,
+        )
+
+    def arrived(pair, side, part):
+        to_partner(pair, side, part, pair, side).wait_recv()
+
+    own.wait()
+    for part in range(2):
+        to_right(1, 0, part, 1).start()
+        to_left(1, 0, part, 1, src_side=0).start()
+        to_partner(0, 0, part, 0, 1).start()
+
+    acc[...] = jnp.zeros_like(acc)
+    lbuf[...] = jnp.zeros_like(lbuf)
+    mbuf[...] = jnp.full(mbuf.shape, -1e30, jnp.float32)
+
+    def compute(pair):
+        keys = kvbuf[pair, :, pl.ds(0, tok), :].reshape(2 * tok, tok)
+        for h, (a0, rows, v0, scale) in enumerate(heads):
+            s = jnp.dot(keys, qt_ref[h], preferred_element_type=jnp.float32)
+            m_old = mbuf[h]
+            m_new = jnp.maximum(m_old, jnp.max(s, axis=0, keepdims=True))
+            p = jnp.exp2((s - m_new) * (scale * LOG2E))
+            shrink = jnp.exp2((m_old - m_new) * (scale * LOG2E))
+            mbuf[h] = m_new
+            lbuf[h] = lbuf[h] * shrink + jnp.sum(p, axis=0, keepdims=True)
+            pb = p.astype(jnp.bfloat16)
+            pv = jnp.dot(
+                kvbuf[pair, 0, pl.ds(tok + v0, rows), :],
+                pb[:tok],
+                preferred_element_type=jnp.float32,
+            ) + jnp.dot(
+                kvbuf[pair, 1, pl.ds(tok + v0, rows), :],
+                pb[tok:],
+                preferred_element_type=jnp.float32,
+            )
+            acc[pl.ds(a0, rows), :] = acc[pl.ds(a0, rows), :] * shrink + pv
+
+    def turn(t, carry):
+        step = t // 2 + 1
+        phase = lax.rem(t, 2)
+        pair = 2 * step - 1
+        for part in range(2):
+
+            @pl.when((phase == part) & (step < last))
+            def _():
+                for side in range(2):
+                    arrived(pair, side, part)
+
+                @pl.when(step < last - 1)
+                def _():
+                    to_right(step + 1, pair, part, pair + 2).start()
+                    to_left(step + 1, pair, part, pair + 2).start()
+
+                @pl.when(step == last - 1)
+                def _():
+                    if part == 0:
+                        to_right(step + 1, pair, 0, 2 * last - 1).start()
+                    else:
+                        to_left(step + 1, pair, 1, 2 * last - 1, dst_side=0).start()
+
+                for side in range(2):
+                    to_partner(pair, side, part, pair + 1, side).start()
+
+        @pl.when(t == 0)
+        def _():
+            for part in range(2):
+                arrived(0, 1, part)
+
+        @pl.when((phase == 0) & (t > 0))
+        def _():
+            for side in range(2):
+                for part in range(2):
+                    arrived(t, side, part)
+
+        @pl.when(t == 2 * last - 1)
+        def _():
+            for part in range(2):
+                arrived(2 * last - 1, 0, part)
+                to_partner(2 * last - 1, 0, part, 2 * last - 1, 1).start()
+            for part in range(2):
+                arrived(2 * last - 1, 1, part)
+
+        compute(t)
+        return carry
+
+    lax.fori_loop(0, 2 * last, turn, 0)
+
+    for w in w_copies:
+        w.wait()
+    for h, (a0, rows, v0, scale) in enumerate(heads):
+        heard = acc[pl.ds(a0, rows), :] / lbuf[h]
+        acc[pl.ds(a0, rows), :] = heard
+    heard = jnp.transpose(acc[...]).astype(jnp.bfloat16)
+    block = tok // 4
+    hbuf[...] = heard.reshape(4, block, heard.shape[1])
+
+    def project(where, owner):
+        pbuf[where] = jnp.dot(
+            hbuf[owner], wbuf[...], preferred_element_type=jnp.float32
+        ).astype(jnp.bfloat16)
+
+    half = block // 2
+    lo, hi = pl.ds(0, half), pl.ds(half, half)
+    project(0, x_far)
+    first_r = _send(pbuf.at[0, lo], xbuf.at[3, lo], xs.at[0], xr.at[0], "tp", x_right)
+    first_l = _send(pbuf.at[0, hi], xbuf.at[3, hi], xs.at[1], xr.at[1], "tp", x_left)
+    first_r.start()
+    first_l.start()
+    project(1, x_right)
+    near_r = _send(pbuf.at[1], xbuf.at[0], xs.at[2], xr.at[2], "tp", x_right)
+    near_r.start()
+    project(2, x_left)
+    near_l = _send(pbuf.at[2], xbuf.at[1], xs.at[3], xr.at[3], "tp", x_left)
+    near_l.start()
+    project(3, tp)
+    first_r.wait_recv()
+    pass_r = _send(xbuf.at[3, lo], xbuf.at[2, lo], xs.at[4], xr.at[4], "tp", x_right)
+    pass_r.start()
+    first_l.wait_recv()
+    pass_l = _send(xbuf.at[3, hi], xbuf.at[2, hi], xs.at[5], xr.at[5], "tp", x_left)
+    pass_l.start()
+
+    for pair in range(2 * last):
+        for side in range(2):
+            rts_ref[pair, side] = kvbuf[pair, side, pl.ds(kv_rows - 16, 16), pl.ds(0, 128)]
+
+    near_r.wait_recv()
+    near_l.wait_recv()
+    pass_r.wait_recv()
+    pass_l.wait_recv()
+    total = (
+        pbuf[3].astype(jnp.float32)
+        + xbuf[0].astype(jnp.float32)
+        + xbuf[1].astype(jnp.float32)
+        + xbuf[2].astype(jnp.float32)
+    )
+    attended = (res_ref[...].astype(jnp.float32) + total).astype(jnp.bfloat16)
+    att_ref[...] = attended
+    wide = attended.astype(jnp.float32)
+    nrm_ref[...] = (
+        wide
+        * lax.rsqrt(jnp.mean(wide * wide, axis=-1, keepdims=True) + norm_eps)
+        * gain_ref[...]
+    ).astype(jnp.bfloat16)
+
+    for c in (first_r, first_l, near_r, near_l, pass_r, pass_l):
+        c.wait_send()
+    for part in range(2):
+        to_right(1, 0, part, 1).wait_send()
+        to_left(1, 0, part, 1, src_side=0).wait_send()
+        to_partner(0, 0, part, 0, 1).wait_send()
+
+    def sent(step, carry):
+        pair = 2 * step - 1
+        for part in range(2):
+
+            @pl.when(step < last - 1)
+            def _():
+                to_right(step + 1, pair, part, pair + 2).wait_send()
+                to_left(step + 1, pair, part, pair + 2).wait_send()
+
+            for side in range(2):
+                to_partner(pair, side, part, pair + 1, side).wait_send()
+        return carry
+
+    lax.fori_loop(1, last, sent, 0)
+    to_right(last, 2 * last - 3, 0, 2 * last - 1).wait_send()
+    to_left(last, 2 * last - 3, 1, 2 * last - 1, dst_side=0).wait_send()
+    for part in range(2):
+        to_partner(2 * last - 1, 0, part, 2 * last - 1, 1).wait_send()
+
+
+def attend(kv_block, queries_t, w_small, w_large, residual, gain, heads, n_sp):
+    pairs = n_sp // 2
+    kv_rows, tok = kv_block.shape
+    width = residual.shape[1]
+    rows = residual.shape[0]
+    n_heads = queries_t.shape[0]
+    vmem = pl.BlockSpec(memory_space=pltpu.VMEM)
+    hbm = pl.BlockSpec(memory_space=pl.ANY)
+    depth = w_small.shape[0] + w_large.shape[0]
+    return pl.pallas_call(
+        functools.partial(attend_kernel, heads),
+        out_shape=(
+            jax.ShapeDtypeStruct((rows, width), jnp.bfloat16),
+            jax.ShapeDtypeStruct((rows, width), jnp.bfloat16),
+            jax.ShapeDtypeStruct((pairs, 2, 16, 128), jnp.bfloat16),
+        ),
+        in_specs=[hbm, vmem, hbm, hbm, vmem, vmem],
+        out_specs=(vmem, vmem, vmem),
+        scratch_shapes=[
+            pltpu.VMEM((pairs, 2, kv_rows, tok), jnp.bfloat16),
+            pltpu.VMEM((depth, width), jnp.bfloat16),
+            pltpu.VMEM((depth, tok), jnp.float32),
+            pltpu.VMEM((n_heads, 1, tok), jnp.float32),
+            pltpu.VMEM((n_heads, 1, tok), jnp.float32),
+            pltpu.VMEM((4, tok // 4, depth), jnp.bfloat16),
+            pltpu.VMEM((4, rows, width), jnp.bfloat16),
+            pltpu.VMEM((4, rows, width), jnp.bfloat16),
+            pltpu.SemaphoreType.DMA((3,)),
+            pltpu.SemaphoreType.DMA((pairs, 2, 2)),
+            pltpu.SemaphoreType.DMA((pairs // 2 + 1, 2, 2)),
+            pltpu.SemaphoreType.DMA((pairs, 2, 2)),
+            pltpu.SemaphoreType.DMA((6,)),
+            pltpu.SemaphoreType.DMA((6,)),
+        ],
+        compiler_params=pltpu.CompilerParams(
+            collective_id=0, has_side_effects=True, vmem_limit_bytes=48 * 1024 * 1024
+        ),
+        name="attend",
+    )(kv_block, queries_t, w_small, w_large, residual, gain)
 
 
 def grid_tables(offset, length, head_size):
@@ -72,68 +370,6 @@
         widened * lax.rsqrt(jnp.mean(widened * widened, axis=-1, keepdims=True) + norm_eps) * gain
     )
     return grid_turn(scaled, tables).astype(jnp.bfloat16)
-
-
-def block_rows(row_count, shard_rows):
-    shards = row_count // shard_rows
-    chosen = 1
-    for factor in range(1, max(1, block_target // shard_rows) + 1):
-        if shards % factor == 0:
-            chosen = factor
-    return chosen * shard_rows
-
-
-def attend_block(state, queries, key_rows, value_rows):
-    largest, weight_sum, accumulated = state
-    head_size = queries.shape[-1]
-    kv_local = queries.shape[1]
-    key_heads = key_rows.reshape(key_rows.shape[0], kv_local, head_size)
-    value_heads = value_rows.reshape(value_rows.shape[0], kv_local, head_size)
-    scores = jnp.einsum(
-        "qgrd,kgd->qgrk", queries, key_heads, preferred_element_type=jnp.float32
-    ) * head_size ** (-0.5)
-    peak_score = jnp.maximum(largest, jnp.max(scores, axis=-1))
-    shrink = jnp.exp(largest - peak_score)
-    weights = jnp.exp(scores - peak_score[..., None])
-    weight_sum = weight_sum * shrink + jnp.sum(weights, axis=-1)
-    accumulated = accumulated * shrink[..., None] + jnp.einsum(
-        "qgrk,kgd->qgrd",
-        weights.astype(jnp.bfloat16),
-        value_heads,
-        preferred_element_type=jnp.float32,
-    )
-    return (peak_score, weight_sum, accumulated)
-
-
-def attend_rows(state, queries, key_rows, value_rows):
-    row_count = key_rows.shape[0]
-    step_rows = block_rows(row_count, queries.shape[0])
-
-    def one_block(block_index, carried):
-        offset = block_index * step_rows
-        return attend_block(
-            carried,
-            queries,
-            lax.dynamic_slice_in_dim(key_rows, offset, step_rows, 0),
-            lax.dynamic_slice_in_dim(value_rows, offset, step_rows, 0),
-        )
-
-    return lax.fori_loop(0, row_count // step_rows, one_block, state)
-
-
-def empty_state(queries):
-    state_shape = queries.shape[:3]
-    return (
-        jnp.full(state_shape, -1e30, jnp.float32),
-        jnp.zeros(state_shape, jnp.float32),
-        jnp.zeros(queries.shape, jnp.float32),
-    )
-
-
-def finish(state):
-    largest, weight_sum, accumulated = state
-    merged = accumulated / weight_sum[..., None]
-    return merged.reshape(merged.shape[0], -1).astype(jnp.bfloat16)
 
 
 def on_device(
@@ -165,38 +401,44 @@
     kv_large = keys_large.shape[1] // HS_LARGE
     asked_small = normed_turn(
         queries_small.reshape(token_rows, -1, HS_SMALL), query_gain_small, tables_small
-    ).reshape(token_rows, kv_small, -1, HS_SMALL)
+    )
     asked_large = normed_turn(
         queries_large.reshape(token_rows, -1, HS_LARGE), query_gain_large, tables_large
-    ).reshape(token_rows, kv_large, -1, HS_LARGE)
+    )
     turned_small = normed_turn(
         keys_small.reshape(token_rows, kv_small, HS_SMALL), key_gain_small, tables_small
     ).reshape(token_rows, -1)
     turned_large = normed_turn(
         keys_large.reshape(token_rows, kv_large, HS_LARGE), key_gain_large, tables_large
     ).reshape(token_rows, -1)
-    key_small, value_small, key_large, value_large = sent_together(
-        (turned_small, values_small, turned_large, values_large), "sp", 0, 1
-    )
-    state_small = attend_rows(empty_state(asked_small), asked_small, key_small, value_small)
-    state_large = attend_rows(empty_state(asked_large), asked_large, key_large, value_large)
-    heard_small = finish(state_small)
-    heard_large = finish(state_large)
-    projected = sent_and_summed(
-        (
-            jnp.dot(heard_small, out_weight_small, preferred_element_type=jnp.float32)
-            + jnp.dot(heard_large, out_weight_large, preferred_element_type=jnp.float32)
-        ).astype(jnp.bfloat16),
-        "tp",
-        0,
-    )
-    attended = (residual_in.astype(jnp.float32) + projected).astype(jnp.bfloat16)
-    widened = attended.astype(jnp.float32)
-    normed = (
-        widened
-        * lax.rsqrt(jnp.mean(widened * widened, axis=-1, keepdims=True) + norm_eps)
-        * norm_gain
-    ).astype(jnp.bfloat16)
+    wide_small = turned_small.shape[1]
+    width = wide_small + turned_large.shape[1]
+    key_block = jnp.concatenate([turned_small, turned_large], axis=1)
+    value_block = jnp.concatenate([values_small, values_large], axis=1).T
+    names = routes.T.reshape(1, -1).astype(jnp.bfloat16)
+    names = jnp.pad(names, ((0, 15), (0, token_rows - names.shape[1])))
+    kv_block = jnp.concatenate([key_block, value_block, names], axis=0)
+    heads, query_parts = [], []
+    for asked, count, size, base in (
+        (asked_small, kv_small, HS_SMALL, 0),
+        (asked_large, kv_large, HS_LARGE, wide_small),
+    ):
+        by_head = jnp.transpose(asked, (1, 2, 0))
+        ratio = asked.shape[1] // count
+        for h in range(asked.shape[1]):
+            at = base + (h // ratio) * size
+            heads.append((base * 2 + h * size, size, at, size ** (-0.5)))
+            query_parts.append(jnp.pad(by_head[h], ((at, width - at - size), (0, 0))))
+    attended, normed, names_all = attend(
+        kv_block,
+        jnp.stack(query_parts),
+        out_weight_small,
+        out_weight_large,
+        residual_in,
+        norm_gain.reshape(1, -1),
+        tuple(heads),
+        lax.axis_size("sp"),
+    )
     local_rows = routes.shape[0]
     top_count = routes.shape[1]
     sp_count = lax.axis_size("sp")

time: 522 us -> 374 us (0.72)
  waiting for transfers between devices: 274 us -> 154 us
  Pallas kernels: 0 us -> 94.9 us
  matrix products: 86.1 us -> 12.2 us
  other arithmetic: 33.7 us -> 7.84 us
  local copies, waits for them, and re-layouts: 30 us -> 16.7 us
    all_gather x1 -> x0, waiting for transfers between devices: 108 us -> none  [sent_together(): lax.all_gather(both, axis, axis=dim, tiled=True)]
    pallas_call x0 -> x1, Pallas kernels: none -> 94.9 us  [attend(): pl.pallas_call(functools.partial(attend_kernel, heads), out_shape=(jax.Sh...]
    dot_general x34 -> x0, matrix products: 72.6 us -> none  [the longest x16 43.6 us: attend_block(): jnp.einsum('qgrd,kgd->qgrk', queries, key_heads, preferred_element_type=j...]
    reduce_sum x18 -> x0, other arithmetic: 28.5 us -> none  [the longest x16 27.2 us: attend_block(): weight_sum = weight_sum * shrink + jnp.sum(weights, axis=-1)]
    all_to_all x1 -> x0, waiting for transfers between devices: 13.6 us -> none  [sent_and_summed(): lax.all_to_all(blocks, axis, split_axis=0, concat_axis=0, tiled=True)]
    dynamic_slice x8 -> x0, local copies, waits for them, and re-layouts: 8.56 us -> none  [one_block(): lax.dynamic_slice_in_dim(value_rows, offset, step_rows, 0)]
    split x1 -> x0, local copies, waits for them, and re-layouts: 5.96 us -> none  [sent_together(): jnp.split(lax.all_gather(both, axis, axis=dim, tiled=True), ends, axis=al...]
  transfers between devices with their start and end apart: 5 -> 3, of which waited for: 5 -> 3; matrix products, arithmetic and copies ran while one was open for 0% -> 0% of each run, Pallas kernels for 0% -> 0%
where the time goes in v1:
time: 374 us; the launch traced here: 373 us
  waiting for transfers between devices  154 us (41%)
  Pallas kernels  94.9 us (25%)
  blocking collectives  59.7 us (16%)
  local copies, waits for them, and re-layouts  16.7 us (4%)
  between operations  13.9 us (4%)
  starting transfers between devices  13.4 us (4%)
  matrix products  12.2 us (3%)
  other arithmetic  7.84 us (2%)
    pallas_call x1, Pallas kernels, attend(): pl.pallas_call(functools.partial(attend_kernel, heads), out_shape=(jax.Sh...  94.9 us
    all_to_all x1, blocking collectives, on_device(): lax.all_to_all(outgoing, 'sp', split_axis=0, concat_axis=0, tiled=True)  59.7 us
    all_to_all x1, waiting for transfers between devices, on_device(): lax.all_to_all(summed, 'sp', split_axis=0, concat_axis=0, tiled=True)  55.5 us
    reduce_scatter x1, waiting for transfers between devices, on_device(): lax.psum_scatter(jnp.einsum('secf,efd->secd', active, expert_down, prefer...  53.5 us
    all_gather x1, waiting for transfers between devices, on_device(): lax.all_gather(lax.all_to_all(outgoing, 'sp', split_axis=0, concat_axis=0...  45.1 us
    all_to_all x1, starting transfers between devices, on_device(): lax.all_to_all(summed, 'sp', split_axis=0, concat_axis=0, tiled=True)  13.2 us
  transfers between devices with their start and end apart: 3, of which 3 were waited for; matrix products, arithmetic and copies ran while one was open for 0% of the time, Pallas kernels for 0%

profile of v1, /device:TPU:33, one launch (start us, length us, event | category | flops | bytes accessed | tf_op | source)
XLA Modules:
  0.0 373.0 jit_solution(10123400130067333635)
XLA Ops:
  6.6 1.1 copy.78
  7.8 0.0 copy-start.12
  7.9 0.8 multiply_multiply_fusion
  8.6 0.3 multiply_cosine_fusion.3
  9.0 0.2 multiply_cosine_fusion.5
  9.2 0.1 copy.77
  9.4 0.1 multiply_multiply_fusion.1
  9.6 0.6 slice_bitcast_fusion.2
  10.2 0.1 copy.71
  10.4 0.1 fusion.35
  10.5 0.1 copy.74
  10.7 0.1 fusion.31
  10.8 0.8 fusion.33
  11.6 2.5 fusion.52
  14.1 0.8 copy.79
  14.8 0.1 eq.54
  15.0 0.1 fusion.49
  15.1 0.2 reduce_window_sum.11
  15.3 0.2 select_reduce_fusion
  15.4 0.1 reduce_sum.82
  15.6 0.1 copy.80
  15.6 0.8 convert_bitcast_fusion.1
  16.4 0.1 convert_element_type.112
  16.5 0.9 copy.75
  17.4 0.9 copy.76
  18.4 0.7 fusion.47
  19.1 0.8 bitcast_dynamic-update-slice_fusion.4
  20.0 1.1 concatenate.40
  21.1 1.2 copy-done.1
  22.3 1.2 copy-done.2
  23.5 94.9 %attend.1 = (bf16[64,2048]{1,0:T(8,128)(2,1)S(1)}, bf16[64,2048]{1,0:T(8,128)(2,1)S(1)}, bf16[16,2,16,128]{3,2,1,0:T(8,128)(2,1)}) custom-call(bf16[528,256]{1,0:T(8,128)(2,1)S(1)} %fusion.22.kv_hbm, bf16[6,256,256]{2,1,0:T(8,128)(2,1)S(1)} %bitcast_dynamic-update-slice_fusion.qt_ref, bf16[256,2048]{1,0:T(8,128)(2,1)S(1)} %copy-done.1, ...), custom_call_target="tpu_custom_call" | custom-call | tf_op jit(solution)/shard_map/attend/pallas_call | solution.py:302
  118.4 0.4 convolution_convert_fusion
  118.9 1.2 reshape.519
  120.1 59.7 %all_to_all.10 = bf16[32,2,4,2048]{3,2,1,0:T(4,128)(2,1)S(1)} all-to-all(bf16[32,2,4,2048]{3,2,1,0:T(4,128)(2,1)} %reshape.519), channel_id=1, replica_groups=mesh['grp'=2,'sp'=32,'tp'=4] {'sp'}, dimensions={0} | all-to-all | bytes 2097152 | tf_op jit(solution)/shard_map/all_to_all | solution.py:463
  179.8 1.6 copy.81
  181.4 0.1 all-gather.2.cloned.1.call-update
  181.4 0.2 reduce-scatter.2.cloned.1.call-start
  181.7 45.1 %all-gather.2.cloned.1.call-done = bf16[128,2,4,2048]{3,0,2,1:T(8,128)(2,1)} async-done(((bf16[32,2,4,2048]{3,0,2,1:T(8,128)(2,1)}), bf16[128,2,4,2048]{3,0,2,1:T(8,128)(2,1)}) %all-gather.2.cloned.1.call-update) | async-done | bytes 4194320 | tf_op jit(solution)/shard_map/all_gather | solution.py:462
  226.8 4.1 %fusion.5 = f32[128,2,4,256]{3,0,2,1:T(8,128)S(1)} fusion(bf16[128,2,4,2048]{3,0,2,1:T(8,128)(2,1)} %all-gather.2.cloned.1.call-done, bf16[2,2048,256]{2,1,0:T(8,128)(2,1)} %param.35), kind=kOutput, calls=%fused_computation.8 | convolution fusion | flops 1073741824 | bytes 7340032 | tf_op jit(solution)/shard_map/secd,edf->secf/dot_general | solution.py:468
  230.9 7.3 %convert_bitcast_fusion = bf16[128,2,4,2048]{3,0,2,1:T(8,128)(2,1)} fusion(bf16[2,256,2048]{2,1,0:T(8,128)(2,1)S(1)} %copy-done, bf16[128,2,4,2048]{3,0,2,1:T(8,128)(2,1)} %all-gather.2.cloned.1.call-done, bf16[2,2048,256]{2,1,0:T(8,128)(2,1)} %param.36, f32[128,2,4,256]{3,0,2,1:T(8,128)S(1)} %fusion.5), kind=kOutput, calls=%fused_computation | convolution fusion | flops 2151153664 | bytes 13631488 | tf_op jit(solution)/shard_map/secf,efd->secd/dot_general | solution.py:474
  238.3 0.1 reduce-scatter.2.cloned.1.call-update
  238.3 53.5 %reduce-scatter.2.cloned.1.call-done = bf16[32,2,4,2048]{3,0,2,1:T(8,128)(2,1)} async-done(((bf16[128,2,4,2048]{3,0,2,1:T(8,128)(2,1)}), bf16[32,2,4,2048]{3,0,2,1:T(8,128)(2,1)}) %reduce-scatter.2.cloned.1.call-update) | async-done | bytes 1048592 | tf_op jit(solution)/shard_map/reduce_scatter | solution.py:473
  291.8 3.1 copy.82
  294.9 13.2 %all-to-all-start.1 = ((bf16[32,2,4,2048]{3,2,1,0:T(4,128)(2,1)}), bf16[32,2,4,2048]{3,2,1,0:T(4,128)(2,1)}, u32[]{:S(2)}, u32[]{:S(2)}) async-start(bf16[32,2,4,2048]{3,2,1,0:T(4,128)(2,1)} %copy.82), calls=%async_computation.2 | async-start | bytes 2097152 | tf_op jit(solution)/shard_map/all_to_all | solution.py:481
  308.1 55.5 %all-to-all-done.1 = bf16[32,2,4,2048]{3,2,1,0:T(4,128)(2,1)} async-done(((bf16[32,2,4,2048]{3,2,1,0:T(4,128)(2,1)}), bf16[32,2,4,2048]{3,2,1,0:T(4,128)(2,1)}, u32[]{:S(2)}, u32[]{:S(2)}) %all-to-all-start.1) | async-done | bytes 1048608 | tf_op jit(solution)/shard_map/all_to_all | solution.py:481
  363.7 1.3 reshape.527
  365.0 0.4 fusion.17
  365.4 0.8 add_convert_fusion
  (50 shorter events, 0.5 us)
Async XLA Ops:
  6.5 224.4 %copy-start = (bf16[2,256,2048]{2,1,0:T(8,128)(2,1)S(1)}, bf16[2,256,2048]{2,1,0:T(8,128)(2,1)}, u32[]{:S(2)}) copy-start(bf16[2,256,2048]{2,1,0:T(8,128)(2,1)} %param.37) | copy-start | bytes 6291460
  6.6 2.7 copy-start.6
  6.6 2.8 copy-start.11
  6.6 220.3 %all-gather.2.cloned.1.call-start = ((), (), s32[]{:S(2)}) async-start(), calls=%async_computation.3 | async-start | bytes 5242880 | tf_op jit(solution)/shard_map/all_gather | solution.py:462
  6.6 3.0 copy-start.10
  7.8 2.4 copy-start.8
  7.8 2.5 copy-start.12
  8.9 1.7 copy-start.5
  10.5 10.6 %copy-start.3 = (bf16[64,2048]{1,0:T(8,128)(2,1)S(1)}, bf16[64,2048]{1,0:T(8,128)(2,1)}, u32[]{:S(2)}) copy-start(bf16[64,2048]{1,0:T(8,128)(2,1)} %res_ref.1) | copy-start | bytes 786436
  10.5 10.6 %copy-start.4 = (f32[2048]{0:T(1024)S(1)}, f32[2048]{0:T(1024)}, u32[]{:S(2)}) copy-start(f32[2048]{0:T(1024)} %param.32) | copy-start | bytes 24580
  21.0 97.4 %copy-start.7 = (bf16[64,256]{1,0:T(8,128)(2,1)S(1)}, bf16[64,256]{1,0:T(8,128)(2,1)}, u32[]{:S(2)}) copy-start(bf16[64,256]{1,0:T(8,128)(2,1)} %fusion.47) | copy-start | bytes 98308
  21.1 1.2 copy-start.1
  22.3 1.2 copy-start.2
  181.4 110.4 %reduce-scatter.2.cloned.1.call-start = ((), (), s32[]{:S(2)}) async-start(), calls=%async_computation.4 | async-start | bytes 5242880 | tf_op jit(solution)/shard_map/reduce_scatter | solution.py:473
  238.3 69.8 %copy-start.9 = (f32[64,2]{0,1:T(2,128)S(1)}, f32[64,2]{0,1:T(2,128)}, u32[]{:S(2)}) copy-start(f32[64,2]{0,1:T(2,128)} %param.34) | copy-start | bytes 1540
  294.9 68.8 %all-to-all-start.1 = ((bf16[32,2,4,2048]{3,2,1,0:T(4,128)(2,1)}), bf16[32,2,4,2048]{3,2,1,0:T(4,128)(2,1)}, u32[]{:S(2)}, u32[]{:S(2)}) async-start(bf16[32,2,4,2048]{3,2,1,0:T(4,128)(2,1)} %copy.82), calls=%async_computation.2 | async-start | bytes 2097152 | tf_op jit(solution)/shard_map/all_to_all | solution.py:481
Sparse Core Ops, SparseCore 0:
  181.6 45.2 all-gather.1
  238.4 53.3 reduce-scatter.1

commit v2 on v1

--- a/solution.py
+++ b/solution.py
@@ -331,6 +331,479 @@
     )(kv_block, queries_t, w_small, w_large, residual, gain)
 
 
+def experts_kernel(
+    x_hbm,
+    att_ref,
+    sel_ref,
+    perm_ref,
+    pick_ref,
+    share_ref,
+    wg_hbm,
+    wu_hbm,
+    wd_hbm,
+    out_ref,
+    xbuf,
+    wg,
+    wu,
+    wd,
+    gbuf,
+    pbuf,
+    rbuf,
+    fbuf,
+    obuf,
+    ret,
+    lsem,
+    rsem,
+    ssem,
+    psem,
+    gr,
+    gs,
+    rr,
+    rs,
+    tr,
+    ts,
+):
+    n_sp = lax.axis_size("sp")
+    n_z = n_sp // 2
+    last = n_z // 2
+    sp = lax.axis_index("sp")
+    tp = lax.axis_index("tp")
+    z = sp // 2
+    core = lax.rem(sp, 2)
+    right = lax.rem(sp + 2, n_sp)
+    left = lax.rem(sp + n_sp - 2, n_sp)
+    partner = sp + 1 - 2 * core
+    x_right = lax.rem(tp + 1, 4)
+    x_left = lax.rem(tp + 3, 4)
+    rows = xbuf.shape[2]
+
+    own = pltpu.make_async_copy(x_hbm, xbuf.at[0, 0], lsem.at[0])
+    own.start()
+    w_copies = [
+        pltpu.make_async_copy(a, b, lsem.at[1 + i])
+        for i, (a, b) in enumerate(((wg_hbm, wg), (wu_hbm, wu), (wd_hbm, wd)))
+    ]
+    for w in w_copies:
+        w.start()
+
+    barrier = pltpu.get_barrier_semaphore()
+
+    def greet(i, carry):
+        pl.semaphore_signal(
+            barrier,
+            inc=1,
+            device_id={"sp": lax.rem(sp + i, n_sp)},
+            device_id_type=pl.DeviceIdType.MESH,
+        )
+        return carry
+
+    lax.fori_loop(1, n_sp, greet, 0)
+    for dev in (x_right, x_left):
+        pl.semaphore_signal(
+            barrier, inc=1, device_id={"tp": dev}, device_id_type=pl.DeviceIdType.MESH
+        )
+    pl.semaphore_wait(barrier, n_sp + 1)
+
+    half = rows // 2
+    parts = (pl.ds(0, half), pl.ds(half, half))
+
+    def at(pair, side, part):
+        return xbuf.at[pair, side, parts[part]]
+
+    def to_right(step, pair, part, dst_pair):
+        return _send(
+            at(pair, 0, part),
+            at(dst_pair, 0, part),
+            ssem.at[step, 0, part],
+            rsem.at[dst_pair, 0, part],
+            "sp",
+            right,
+        )
+
+    def to_left(step, pair, part, dst_pair, src_side=1, dst_side=1):
+        return _send(
+            at(pair, src_side, part),
+            at(dst_pair, dst_side, part),
+            ssem.at[step, 1, part],
+            rsem.at[dst_pair, dst_side, part],
+            "sp",
+            left,
+        )
+
+    def to_partner(pair, side, part, dst_pair, dst_side):
+        return _send(
+            at(pair, side, part),
+            at(dst_pair, dst_side, part),
+            psem.at[dst_pair, dst_side, part],
+            rsem.at[dst_pair, dst_side, part],
+            "sp",
+            partner,
+        )
+
+    def arrived(pair, side, part):
+        to_partner(pair, side, part, pair, side).wait_recv()
+
+    def share_right(c):
+        return _send(gbuf.at[c, 0], gbuf.at[c, 1], gs.at[c, 0], gr.at[c, 0], "tp", x_right)
+
+    def share_left(c):
+        return _send(gbuf.at[c, 0], gbuf.at[c, 2], gs.at[c, 1], gr.at[c, 1], "tp", x_left)
+
+    def pass_right(c):
+        return _send(
+            gbuf.at[c, 1, 0], gbuf.at[c, 3, 0], gs.at[c, 2], gr.at[c, 2], "tp", x_right
+        )
+
+    def pass_left(c):
+        return _send(gbuf.at[c, 2, 1], gbuf.at[c, 3, 1], gs.at[c, 3], gr.at[c, 3], "tp", x_left)
+
+    def far_right(c):
+        return _send(pbuf.at[c, 3, 0], rbuf.at[c, 0], rs.at[c, 0], rr.at[c, 0], "tp", x_right)
+
+    def far_left(c):
+        return _send(pbuf.at[c, 3, 1], rbuf.at[c, 1], rs.at[c, 1], rr.at[c, 1], "tp", x_left)
+
+    def near_right(c):
+        return _send(pbuf.at[c, 2], fbuf.at[c, 0], rs.at[c, 2], rr.at[c, 2], "tp", x_right)
+
+    def near_left(c):
+        return _send(pbuf.at[c, 1], fbuf.at[c, 1], rs.at[c, 3], rr.at[c, 3], "tp", x_left)
+
+    own.wait()
+    for part in range(2):
+        to_right(1, 0, part, 1).start()
+        to_left(1, 0, part, 1, src_side=0).start()
+        to_partner(0, 0, part, 0, 1).start()
+
+    def run_experts(c):
+        for e in range(2):
+            x = gbuf[c, :, e].reshape(64, gbuf.shape[4])
+            gate = jnp.dot(x, wg[e], preferred_element_type=jnp.float32)
+            up = jnp.dot(x, wu[e], preferred_element_type=jnp.float32)
+            active = (gate / (1.0 + jnp.exp(-gate)) * up).astype(jnp.bfloat16)
+            term = jnp.dot(active, wd[e], preferred_element_type=jnp.float32)
+            pbuf[c, :, e] = term.astype(jnp.bfloat16).reshape(4, 16, gbuf.shape[4])
+
+    def gather_turn(c, carry):
+        step = c + 1
+        pair = 2 * step - 1
+
+        @pl.when(step < last)
+        def _():
+            for part in range(2):
+                for side in range(2):
+                    arrived(pair, side, part)
+
+                @pl.when(step < last - 1)
+                def _():
+                    to_right(step + 1, pair, part, pair + 2).start()
+                    to_left(step + 1, pair, part, pair + 2).start()
+
+                @pl.when(step == last - 1)
+                def _():
+                    if part == 0:
+                        to_right(step + 1, pair, 0, 2 * last - 1).start()
+                    else:
+                        to_left(step + 1, pair, 1, 2 * last - 1, dst_side=0).start()
+
+                for side in range(2):
+                    to_partner(pair, side, part, pair + 1, side).start()
+
+        @pl.when(step == last)
+        def _():
+            for part in range(2):
+                arrived(2 * last - 1, 0, part)
+                to_partner(2 * last - 1, 0, part, 2 * last - 1, 1).start()
+
+        @pl.when(c == 0)
+        def _():
+            for part in range(2):
+                arrived(0, 1, part)
+
+        @pl.when((c > 0) & (c < last))
+        def _():
+            for side in range(2):
+                for part in range(2):
+                    arrived(2 * c, side, part)
+
+        @pl.when(step == last)
+        def _():
+            for part in range(2):
+                arrived(2 * last - 1, 1, part)
+
+        @pl.when(c < last)
+        def _():
+            tokens = xbuf[pl.ds(2 * c, 2)].reshape(4 * rows, xbuf.shape[3])
+            chosen = jnp.dot(sel_ref[c], tokens, preferred_element_type=jnp.float32)
+            gbuf[c, 0] = chosen.astype(jnp.bfloat16).reshape(2, 16, xbuf.shape[3])
+            share_right(c).start()
+            share_left(c).start()
+
+        @pl.when((c >= 1) & (c < last + 1))
+        def _():
+            share_right(c - 1).wait_recv()
+            pass_right(c - 1).start()
+            share_left(c - 1).wait_recv()
+            pass_left(c - 1).start()
+
+        @pl.when(c == 2)
+        def _():
+            for w in w_copies:
+                w.wait()
+
+        @pl.when(c >= 2)
+        def _():
+            pass_right(c - 2).wait_recv()
+            pass_left(c - 2).wait_recv()
+            run_experts(c - 2)
+
+        return carry
+
+    lax.fori_loop(0, last + 2, gather_turn, 0)
+
+    def home(c, q):
+        if q == 0:
+            return lax.rem(z - c + n_z, n_z) * 2 + 1 - core, 2 * c, 0
+        if q == 1:
+            return lax.rem(z + c, n_z) * 2 + 1 - core, 2 * c, 1
+        if q == 2:
+            return lax.rem(z - c - 1 + n_z, n_z) * 2 + core, 2 * c + 1, 0
+        return lax.rem(z + c + 1, n_z) * 2 + core, 2 * c + 1, 1
+
+    def give(c, q):
+        dev, pair, side = home(c, q)
+        return _send(
+            obuf.at[c, q], ret.at[pair, side], ts.at[c, q], tr.at[pair, side], "sp", dev
+        )
+
+    def give_last():
+        dev = lax.rem(z + last, n_z) * 2 + 1 - core
+        return _send(
+            obuf.at[last - 1, 3],
+            ret.at[2 * last - 1, 1],
+            ts.at[last - 1, 3],
+            tr.at[2 * last - 1, 1],
+            "sp",
+            dev,
+        )
+
+    width = fbuf.shape[4]
+
+    def return_turn(i, carry):
+        @pl.when(i < last)
+        def _():
+            c = last - 1 - i
+            far_right(c).start()
+            far_left(c).start()
+
+        @pl.when((i >= 1) & (i < last + 1))
+        def _():
+            c = last - i
+            far_right(c).wait_recv()
+            pbuf[c, 2, 0] = (
+                pbuf[c, 2, 0].astype(jnp.float32) + rbuf[c, 0].astype(jnp.float32)
+            ).astype(jnp.bfloat16)
+            near_right(c).start()
+            far_left(c).wait_recv()
+            pbuf[c, 1, 1] = (
+                pbuf[c, 1, 1].astype(jnp.float32) + rbuf[c, 1].astype(jnp.float32)
+            ).astype(jnp.bfloat16)
+            near_left(c).start()
+
+        @pl.when(i >= 2)
+        def _():
+            c = last + 1 - i
+            near_right(c).wait_recv()
+            near_left(c).wait_recv()
+            total = (
+                pbuf[c, 0].astype(jnp.float32)
+                + fbuf[c, 0].astype(jnp.float32)
+                + fbuf[c, 1].astype(jnp.float32)
+            )
+            total = total.astype(jnp.bfloat16).reshape(32, width)
+            split = jnp.concatenate([total[:, : width // 2], total[:, width // 2 :]], axis=0)
+            ordered = jnp.dot(perm_ref[...], split, preferred_element_type=jnp.float32)
+            obuf[c] = ordered.astype(jnp.bfloat16).reshape(4, 16, width // 2)
+
+            @pl.when(c > 0)
+            def _():
+                give(c, 0).start()
+
+            @pl.when(c == 0)
+            def _():
+                ret[0, 0] = obuf[0, 0]
+
+            give(c, 1).start()
+            give(c, 2).start()
+
+            @pl.when(c < last - 1)
+            def _():
+                give(c, 3).start()
+
+            @pl.when(c == last - 1)
+            def _():
+                give_last().start()
+
+        return carry
+
+    lax.fori_loop(0, last + 2, return_turn, 0)
+
+    for part in range(2):
+        to_right(1, 0, part, 1).wait_send()
+        to_left(1, 0, part, 1, src_side=0).wait_send()
+        to_partner(0, 0, part, 0, 1).wait_send()
+
+    def sent(step, carry):
+        pair = 2 * step - 1
+        for part in range(2):
+
+            @pl.when(step < last - 1)
+            def _():
+                to_right(step + 1, pair, part, pair + 2).wait_send()
+                to_left(step + 1, pair, part, pair + 2).wait_send()
+
+            for side in range(2):
+                to_partner(pair, side, part, pair + 1, side).wait_send()
+        return carry
+
+    lax.fori_loop(1, last, sent, 0)
+    to_right(last, 2 * last - 3, 0, 2 * last - 1).wait_send()
+    to_left(last, 2 * last - 3, 1, 2 * last - 1, dst_side=0).wait_send()
+    for part in range(2):
+        to_partner(2 * last - 1, 0, part, 2 * last - 1, 1).wait_send()
+
+    def left_all(c, carry):
+        for copy in (share_right, share_left, pass_right, pass_left):
+            copy(c).wait_send()
+        for copy in (far_right, far_left, near_right, near_left):
+            copy(c).wait_send()
+        return carry
+
+    lax.fori_loop(0, last, left_all, 0)
+
+    def came(i, carry):
+        c = last - 1 - i
+
+        @pl.when(c > 0)
+        def _():
+            give(c, 0).wait_recv()
+
+        for q in (1, 2, 3):
+            give(c, q).wait_recv()
+        return carry
+
+    lax.fori_loop(0, last, came, 0)
+
+    back = ret[...].reshape(ret.shape[0] * 32, width // 2)
+    picked = jnp.dot(pick_ref[...], back, preferred_element_type=jnp.float32)
+    out = att_ref[...].astype(jnp.float32)
+    lo = picked[:rows] * share_ref[:, 0:1] + picked[rows : 2 * rows] * share_ref[:, 1:2]
+    hi = (
+        picked[2 * rows : 3 * rows] * share_ref[:, 0:1]
+        + picked[3 * rows :] * share_ref[:, 1:2]
+    )
+    out_ref[:, : width // 2] = (out[:, : width // 2] + lo).astype(jnp.bfloat16)
+    out_ref[:, width // 2 :] = (out[:, width // 2 :] + hi).astype(jnp.bfloat16)
+
+    def gone(c, carry):
+        @pl.when(c > 0)
+        def _():
+            give(c, 0).wait_send()
+
+        for q in (1, 2, 3):
+            give(c, q).wait_send()
+        return carry
+
+    lax.fori_loop(0, last, gone, 0)
+
+
+def run_layer_experts(normed, attended, sel, perm, pick, shares, gate, up, down, n_sp):
+    pairs = n_sp // 2
+    chunks = pairs // 2
+    rows, width = normed.shape
+    vmem = pl.BlockSpec(memory_space=pltpu.VMEM)
+    hbm = pl.BlockSpec(memory_space=pl.ANY)
+    bf16 = jnp.bfloat16
+    dma = pltpu.SemaphoreType.DMA
+    return pl.pallas_call(
+        experts_kernel,
+        out_shape=jax.ShapeDtypeStruct((rows, width), bf16),
+        in_specs=[hbm, vmem, vmem, vmem, vmem, vmem, hbm, hbm, hbm],
+        out_specs=vmem,
+        scratch_shapes=[
+            pltpu.VMEM((pairs, 2, rows, width), bf16),
+            pltpu.VMEM(gate.shape, bf16),
+            pltpu.VMEM(up.shape, bf16),
+            pltpu.VMEM(down.shape, bf16),
+            pltpu.VMEM((chunks, 4, 2, 16, width), bf16),
+            pltpu.VMEM((chunks, 4, 2, 16, width), bf16),
+            pltpu.VMEM((chunks, 2, 16, width), bf16),
+            pltpu.VMEM((chunks, 2, 2, 16, width), bf16),
+            pltpu.VMEM((chunks, 4, 16, width // 2), bf16),
+            pltpu.VMEM((pairs, 2, 16, width // 2), bf16),
+            dma((4,)),
+            dma((pairs, 2, 2)),
+            dma((chunks + 1, 2, 2)),
+            dma((pairs, 2, 2)),
+            dma((chunks, 4)),
+            dma((chunks, 4)),
+            dma((chunks, 4)),
+            dma((chunks, 4)),
+            dma((pairs, 2)),
+            dma((chunks, 4)),
+        ],
+        compiler_params=pltpu.CompilerParams(
+            collective_id=1, has_side_effects=True, vmem_limit_bytes=56 * 1024 * 1024
+        ),
+        name="experts",
+    )(normed, attended, sel, perm, pick, shares, gate, up, down)
+
+
+def experts_of(normed, attended, names_all, routes, route_scores, gate, up, down):
+    n_sp = lax.axis_size("sp")
+    n_z = n_sp // 2
+    last = n_z // 2
+    pairs = n_sp // 2
+    chunks = pairs // 2
+    rows = routes.shape[0]
+    sp = lax.axis_index("sp")
+    bf16 = jnp.bfloat16
+    names = names_all[:, :, 0, :].reshape(n_sp, 2, rows)
+    mine = (2 * sp + jnp.arange(2)).astype(bf16)
+    member = jnp.any(names[:, None] == mine[None, :, None, None], axis=2)
+    before = (jnp.arange(rows)[:, None] < jnp.arange(rows)[None, :]).astype(bf16)
+    rank = jnp.einsum(
+        "bet,tu->beu", member.astype(bf16), before, preferred_element_type=jnp.float32
+    )
+    seats = jnp.arange(4, dtype=jnp.float32)
+    seated = member[:, :, None] & (rank[:, :, None] == seats[None, None, :, None])
+    seated = seated.reshape(chunks, 4, 2, 4, rows).transpose(0, 2, 1, 3, 4)
+    same_block = jnp.arange(4)[:, None, None, None] == jnp.arange(4)[None, None, :, None]
+    sel = (seated[:, :, :, :, None] & same_block[None, None]).astype(bf16)
+    sel = sel.reshape(chunks, 32, 4 * rows)
+    out_row = jnp.arange(64)
+    block, piece, slot = out_row // 16, (out_row // 8) % 2, out_row % 8
+    in_row = piece * 32 + (slot // 4) * 16 + block * 4 + slot % 4
+    perm = (in_row[:, None] == jnp.arange(64)[None, :]).astype(bf16)
+    same = routes[:, :, None, None] == routes[None, None, :, :]
+    earlier = jnp.arange(rows)[:, None, None, None] > jnp.arange(rows)[None, None, :, None]
+    own_rank = jnp.sum((same & earlier).astype(jnp.int32), axis=(2, 3))
+    host = routes // 2
+    away = (sp // 2 - host // 2 + n_z) % n_z
+    other = (host % 2 != sp % 2).astype(jnp.int32)
+    step = jnp.minimum(away, n_z - away)
+    edge = (away == 0) | (away == last)
+    pair = jnp.where(away == 0, 0, jnp.where(away == last, 2 * last - 1, 2 * step - 1 + other))
+    side = jnp.where(edge, other, (away < last).astype(jnp.int32))
+    base = (pair * 2 + side) * 16 + (routes % 2) * 4 + own_rank
+    seats_back = jnp.concatenate([base[:, 0], base[:, 1], base[:, 0] + 8, base[:, 1] + 8])
+    pick = (seats_back[:, None] == jnp.arange(pairs * 32)[None, :]).astype(bf16)
+    shares = route_scores / jnp.sum(route_scores, axis=1, keepdims=True)
+    return run_layer_experts(
+        normed, attended, sel, perm, pick, shares, gate, up, down, n_sp
+    )
+
+
 def grid_tables(offset, length, head_size):
     places = offset + jnp.arange(length, dtype=jnp.int32)
     grid_rows = (places // GRID_W).astype(jnp.float32)
@@ -439,53 +912,16 @@
         tuple(heads),
         lax.axis_size("sp"),
     )
-    local_rows = routes.shape[0]
-    top_count = routes.shape[1]
-    sp_count = lax.axis_size("sp")
-    local_experts = expert_gate.shape[0]
-    expert_count = local_experts * sp_count
-    capacity = max(2, (2 * top_count * local_rows + expert_count - 1) // expert_count)
-    flat_routes = routes.reshape(-1)
-    member = (flat_routes[:, None] == jnp.arange(expert_count, dtype=jnp.int32)[None, :]).astype(
-        jnp.int32
-    )
-    ranks = jnp.sum((jnp.cumsum(member, axis=0) - member) * member, axis=1)
-    slots = flat_routes * capacity + ranks
-    picker = (
-        slots[:, None] == jnp.arange(expert_count * capacity, dtype=jnp.int32)[None, :]
-    ).astype(jnp.bfloat16)
-    placer = jnp.sum(picker.reshape(local_rows, top_count, -1), axis=1)
-    outgoing = jnp.einsum("ts,td->sd", placer, normed, preferred_element_type=jnp.float32).astype(
-        jnp.bfloat16
-    )
-    outgoing = outgoing.reshape(sp_count, local_experts, capacity, -1)
-    everyone = lax.all_gather(
-        lax.all_to_all(outgoing, "sp", split_axis=0, concat_axis=0, tiled=True),
-        "tp",
-        axis=0,
-        tiled=True,
-    )
-    gate_out = jnp.einsum(
-        "secd,edf->secf", everyone, expert_gate, preferred_element_type=jnp.float32
-    )
-    up_out = jnp.einsum("secd,edf->secf", everyone, expert_up, preferred_element_type=jnp.float32)
-    active = (jax.nn.silu(gate_out) * up_out).astype(jnp.bfloat16)
-    summed = lax.psum_scatter(
-        jnp.einsum(
-            "secf,efd->secd", active, expert_down, preferred_element_type=jnp.float32
-        ).astype(jnp.bfloat16),
-        "tp",
-        scatter_dimension=0,
-        tiled=True,
-    )
-    returned = lax.all_to_all(summed, "sp", split_axis=0, concat_axis=0, tiled=True)
-    back_rows = returned.reshape(expert_count * capacity, -1)
-    chosen_rows = jnp.dot(picker, back_rows, preferred_element_type=jnp.float32).reshape(
-        local_rows, top_count, -1
-    )
-    shares = route_scores / jnp.sum(route_scores, axis=1, keepdims=True)
-    mixed = jnp.sum(chosen_rows * shares[:, :, None], axis=1)
-    return (attended.astype(jnp.float32) + mixed).astype(jnp.bfloat16)
+    return experts_of(
+        normed,
+        attended,
+        names_all,
+        routes,
+        route_scores,
+        expert_gate,
+        expert_up,
+        expert_down,
+    )
 
 
 def solution(mesh):

time: 374 us -> 236 us (0.63)
  waiting for transfers between devices: 154 us -> 0 us
  Pallas kernels: 94.9 us -> 217 us
  blocking collectives: 59.7 us -> 0 us
  starting transfers between devices: 13.4 us -> 0 us
  between operations: 13.9 us -> 0.53 us
  matrix products: 12.2 us -> 0.13 us
  local copies, waits for them, and re-layouts: 16.7 us -> 8.5 us
    pallas_call x0 -> x1, Pallas kernels: none -> 122 us  [run_layer_experts(): pl.pallas_call(experts_kernel, out_shape=jax.ShapeDtypeStruct((rows, widt...]
    all_to_all x1 -> x0, blocking collectives: 59.7 us -> none  [on_device(): lax.all_to_all(outgoing, 'sp', split_axis=0, concat_axis=0, tiled=True)]
    all_to_all x1 -> x0, waiting for transfers between devices: 55.5 us -> none  [on_device(): lax.all_to_all(summed, 'sp', split_axis=0, concat_axis=0, tiled=True)]
    reduce_scatter x1 -> x0, waiting for transfers between devices: 53.5 us -> none  [on_device(): lax.psum_scatter(jnp.einsum('secf,efd->secd', active, expert_down, prefer...]
    all_gather x1 -> x0, waiting for transfers between devices: 45.1 us -> none  [on_device(): lax.all_gather(lax.all_to_all(outgoing, 'sp', split_axis=0, concat_axis=0...]
    all_to_all x1 -> x0, starting transfers between devices: 13.2 us -> none  [on_device(): lax.all_to_all(summed, 'sp', split_axis=0, concat_axis=0, tiled=True)]
    dot_general x4 -> x1, matrix products: 12.2 us -> 0.13 us  [experts_of(): jnp.einsum('bet,tu->beu', member.astype(bf16), before, preferred_element_...]
  transfers between devices with their start and end apart: 3 -> 0, of which waited for: 3 -> 0; matrix products, arithmetic and copies ran while one was open for 0% -> 0% of each run, Pallas kernels for 0% -> 0%
where the time goes in v2:
time: 236 us; the launch traced here: 235 us
  Pallas kernels  217 us (92%)
  other arithmetic  9.3 us (4%)
  local copies, waits for them, and re-layouts  8.5 us (4%)
    pallas_call x1, Pallas kernels, run_layer_experts(): pl.pallas_call(experts_kernel, out_shape=jax.ShapeDtypeStruct((rows, widt...  122 us
    pallas_call x1, Pallas kernels, attend(): pl.pallas_call(functools.partial(attend_kernel, heads), out_shape=(jax.Sh...  94.4 us
    unnamed x38, local copies, waits for them, and re-layouts  5.47 us

profile of v2, /device:TPU:33, one launch (start us, length us, event | category | flops | bytes accessed | tf_op | source)
XLA Modules:
  0.0 235.2 jit_solution(16367712575481032376)
XLA Ops:
  0.0 0.3 multiply_cosine_fusion.3
  0.4 0.2 copy-done.10
  0.6 1.0 copy.64
  1.6 0.7 multiply_multiply_fusion
  2.4 0.0 copy-start.8
  2.4 0.0 copy-start.12
  2.5 0.2 multiply_cosine_fusion.5
  2.7 0.0 copy-start.6
  2.7 0.0 copy-start.13
  2.7 0.1 copy.63
  2.9 0.1 multiply_multiply_fusion.1
  3.1 0.0 copy-start
  3.2 0.0 copy-start.1
  3.2 0.0 copy-start.4
  3.2 0.0 copy-start.5
  3.3 0.1 copy.57
  3.4 0.1 fusion.15
  3.6 0.1 copy.60
  3.7 0.1 fusion.11
  3.8 0.1 fusion.13
  3.9 2.4 %fusion.27 = (bf16[256,32]{1,0:T(8,128)(2,1)S(1)}, bf16[256,32]{1,0:T(8,128)(2,1)S(1)}, bf16[256,32]{1,0:T(8,128)(2,1)S(1)}, bf16[256,32]{1,0:T(8,128)(2,1)}) fusion(f32[256,1,128]{2,0,1:T(8,128)S(1)} %fusion.13, f32[32]{0:T(128)} %copy-done.10, f32[256]{0:T(256)S(1)} %get-tuple-element.59, f32[256]{0:T(256)S(1)} %get-tuple-element.60), kind=kLoop, calls=%fused_computation.65 | loop fusion | flops 147456 | bytes 198784 | tf_op jit(solution)/shard_map/concatenate | solution.py:831
  6.4 1.0 concatenate.43
  7.4 0.9 convert_reduce_fusion
  8.3 0.8 fusion.41
  9.1 0.1 convert_element_type.113
  9.2 0.9 copy.61
  10.2 0.9 copy.62
  11.2 0.0 copy-start.9
  11.2 94.4 %attend.1 = (bf16[64,2048]{1,0:T(8,128)(2,1)S(1)}, bf16[64,2048]{1,0:T(8,128)(2,1)S(1)}, bf16[16,2,16,128]{3,2,1,0:T(8,128)(2,1)S(1)}) custom-call(bf16[528,256]{1,0:T(8,128)(2,1)S(1)} %fusion.2.kv_hbm, bf16[6,256,256]{2,1,0:T(8,128)(2,1)S(1)} %bitcast_dynamic-update-slice_fusion.qt_ref, bf16[256,2048]{1,0:T(8,128)(2,1)S(1)} %copy-done, ...), custom_call_target="tpu_custom_call" | custom-call | tf_op jit(solution)/shard_map/attend/pallas_call | solution.py:302
  105.6 0.7 copy-done.2
  106.3 0.7 copy-done.3
  107.0 0.1 slice_reduce_fusion
  107.1 0.1 eq.109
  107.2 0.1 compare_reduce_fusion
  107.3 0.1 convolution_bitcast_fusion
  107.4 0.1 fusion.24
  107.5 0.1 and.179
  107.6 0.2 and.180
  107.9 0.1 and.181
  108.0 0.1 and.182
  108.1 0.7 and_convert_fusion.sel_ref
  108.8 0.1 pad_add_fusion
  108.9 0.8 fusion.1.pick_ref
  109.7 0.1 copy.69
  109.8 0.7 broadcast_divide_fusion.share_ref
  110.5 0.7 fusion.31.perm_ref
  111.2 122.3 %experts.1 = bf16[64,2048]{1,0:T(8,128)(2,1)} custom-call(bf16[64,2048]{1,0:T(8,128)(2,1)} %copy-done.3, bf16[64,2048]{1,0:T(8,128)(2,1)} %copy-done.2, bf16[8,32,256]{2,1,0:T(8,128)(2,1)} %and_convert_fusion.sel_ref, bf16[64,64]{1,0:T(8,128)(2,1)} %fusion.31.perm_ref, bf16[256,512]{1,0:T(8,128)(2,1)} %fusion.1.pick_ref, ...), custom_call_target="tpu_custom_call" | custom-call | tf_op jit(solution)/shard_map/experts/pallas_call | solution.py:728
  233.5 1.7 copy.82
  (51 shorter events, 0.5 us)
Async XLA Ops:
  0.0 2.7 %copy-start.7 = (bf16[256,256]{1,0:T(8,128)(2,1)S(1)}, bf16[256,256]{1,0:T(8,128)(2,1)}, u32[]{:S(2)}) copy-start(bf16[256,256]{1,0:T(8,128)(2,1)} %param.19) | copy-start | bytes 393220
  0.0 2.9 %copy-start.11 = (f32[64]{0:T(128)S(1)}, f32[64]{0:T(128)}, u32[]{:S(2)}) copy-start(f32[64]{0:T(128)} %param.25) | copy-start | bytes 772
  0.0 0.5 copy-start.10
  2.4 0.9 copy-start.8
  2.4 1.0 copy-start.12
  2.7 1.0 copy-start.6
  2.7 1.1 copy-start.13
  3.1 8.0 %copy-start = (bf16[256,2048]{1,0:T(8,128)(2,1)S(1)}, bf16[256,2048]{1,0:T(8,128)(2,1)}, u32[]{:S(2)}) copy-start(bf16[256,2048]{1,0:T(8,128)(2,1)} %ws_hbm.1) | copy-start | bytes 3145732
  3.2 8.0 %copy-start.1 = (bf16[256,2048]{1,0:T(8,128)(2,1)S(1)}, bf16[256,2048]{1,0:T(8,128)(2,1)}, u32[]{:S(2)}) copy-start(bf16[256,2048]{1,0:T(8,128)(2,1)} %wl_hbm.1) | copy-start | bytes 3145732
  3.2 8.0 %copy-start.4 = (bf16[64,2048]{1,0:T(8,128)(2,1)S(1)}, bf16[64,2048]{1,0:T(8,128)(2,1)}, u32[]{:S(2)}) copy-start(bf16[64,2048]{1,0:T(8,128)(2,1)} %res_ref.1) | copy-start | bytes 786436
  3.2 8.0 %copy-start.5 = (f32[2048]{0:T(1024)S(1)}, f32[2048]{0:T(1024)}, u32[]{:S(2)}) copy-start(f32[2048]{0:T(1024)} %param.32) | copy-start | bytes 24580
  11.2 98.5 %copy-start.9 = (f32[64,2]{0,1:T(2,128)S(1)}, f32[64,2]{0,1:T(2,128)}, u32[]{:S(2)}) copy-start(f32[64,2]{0,1:T(2,128)} %param.34) | copy-start | bytes 1540
  105.6 0.7 copy-start.2
  106.3 0.7 copy-start.3

commit v3 on v2

--- a/solution.py
+++ b/solution.py
@@ -12,6 +12,7 @@
 LOG2E = 1.4426950408889634
 theta_base = 10000.0
 norm_eps = 1e-06
+return_lag = 5
 
 
 def _send(src, dst, ssem, rsem, axis, dev):
@@ -484,7 +485,7 @@
             term = jnp.dot(active, wd[e], preferred_element_type=jnp.float32)
             pbuf[c, :, e] = term.astype(jnp.bfloat16).reshape(4, 16, gbuf.shape[4])
 
-    def gather_turn(c, carry):
+    def gather_turn(c):
         step = c + 1
         pair = 2 * step - 1
 
@@ -551,15 +552,11 @@
             for w in w_copies:
                 w.wait()
 
-        @pl.when(c >= 2)
+        @pl.when((c >= 2) & (c < last + 2))
         def _():
             pass_right(c - 2).wait_recv()
             pass_left(c - 2).wait_recv()
             run_experts(c - 2)
-
-        return carry
-
-    lax.fori_loop(0, last + 2, gather_turn, 0)
 
     def home(c, q):
         if q == 0:
@@ -589,16 +586,10 @@
 
     width = fbuf.shape[4]
 
-    def return_turn(i, carry):
-        @pl.when(i < last)
-        def _():
-            c = last - 1 - i
-            far_right(c).start()
-            far_left(c).start()
-
+    def return_turn(i):
         @pl.when((i >= 1) & (i < last + 1))
         def _():
-            c = last - i
+            c = i - 1
             far_right(c).wait_recv()
             pbuf[c, 2, 0] = (
                 pbuf[c, 2, 0].astype(jnp.float32) + rbuf[c, 0].astype(jnp.float32)
@@ -610,9 +601,14 @@
             ).astype(jnp.bfloat16)
             near_left(c).start()
 
+        @pl.when((i >= 0) & (i < last))
+        def _():
+            far_right(i).start()
+            far_left(i).start()
+
         @pl.when(i >= 2)
         def _():
-            c = last + 1 - i
+            c = i - 2
             near_right(c).wait_recv()
             near_left(c).wait_recv()
             total = (
@@ -644,9 +640,12 @@
             def _():
                 give_last().start()
 
+    def turn(t, carry):
+        gather_turn(t)
+        return_turn(t - return_lag)
         return carry
 
-    lax.fori_loop(0, last + 2, return_turn, 0)
+    lax.fori_loop(0, last + return_lag + 2, turn, 0)
 
     for part in range(2):
         to_right(1, 0, part, 1).wait_send()
@@ -682,7 +681,7 @@
     lax.fori_loop(0, last, left_all, 0)
 
     def came(i, carry):
-        c = last - 1 - i
+        c = i
 
         @pl.when(c > 0)
         def _():

time: 236 us -> 242 us (1.025)
  Pallas kernels: 217 us -> 223 us
    pallas_call x1, Pallas kernels: 122 us -> 128 us  [run_layer_experts(): pl.pallas_call(experts_kernel, out_shape=jax.ShapeDtypeStruct((rows, widt...]
where the time goes in v3:
time: 242 us; the launch traced here: 241 us
  Pallas kernels  223 us (92%)
  other arithmetic  9.3 us (4%)
  local copies, waits for them, and re-layouts  8.5 us (4%)
    pallas_call x1, Pallas kernels, run_layer_experts(): pl.pallas_call(experts_kernel, out_shape=jax.ShapeDtypeStruct((rows, widt...  128 us
    pallas_call x1, Pallas kernels, attend(): pl.pallas_call(functools.partial(attend_kernel, heads), out_shape=(jax.Sh...  94.4 us
    unnamed x38, local copies, waits for them, and re-layouts  5.47 us

profile of v3, /device:TPU:33, one launch (start us, length us, event | category | flops | bytes accessed | tf_op | source)
XLA Modules:
  0.0 241.3 jit_solution(8935304922221784593)
XLA Ops:
  0.0 0.3 multiply_cosine_fusion.3
  0.4 0.2 copy-done.10
  0.6 1.0 copy.64
  1.6 0.7 multiply_multiply_fusion
  2.4 0.0 copy-start.8
  2.4 0.0 copy-start.12
  2.5 0.2 multiply_cosine_fusion.5
  2.7 0.0 copy-start.6
  2.7 0.0 copy-start.13
  2.7 0.1 copy.63
  2.9 0.1 multiply_multiply_fusion.1
  3.1 0.0 copy-start
  3.2 0.0 copy-start.1
  3.2 0.0 copy-start.4
  3.2 0.0 copy-start.5
  3.3 0.1 copy.57
  3.4 0.1 fusion.15
  3.6 0.1 copy.60
  3.7 0.1 fusion.11
  3.8 0.1 fusion.13
  3.9 2.4 %fusion.27 = (bf16[256,32]{1,0:T(8,128)(2,1)S(1)}, bf16[256,32]{1,0:T(8,128)(2,1)S(1)}, bf16[256,32]{1,0:T(8,128)(2,1)S(1)}, bf16[256,32]{1,0:T(8,128)(2,1)}) fusion(f32[256,1,128]{2,0,1:T(8,128)S(1)} %fusion.13, f32[32]{0:T(128)} %copy-done.10, f32[256]{0:T(256)S(1)} %get-tuple-element.59, f32[256]{0:T(256)S(1)} %get-tuple-element.60), kind=kLoop, calls=%fused_computation.65 | loop fusion | flops 147456 | bytes 198784 | tf_op jit(solution)/shard_map/concatenate | solution.py:830
  6.4 1.0 concatenate.43
  7.4 0.9 convert_reduce_fusion
  8.3 0.8 fusion.41
  9.1 0.1 convert_element_type.113
  9.2 0.9 copy.61
  10.2 0.9 copy.62
  11.2 0.0 copy-start.9
  11.2 94.4 %attend.1 = (bf16[64,2048]{1,0:T(8,128)(2,1)S(1)}, bf16[64,2048]{1,0:T(8,128)(2,1)S(1)}, bf16[16,2,16,128]{3,2,1,0:T(8,128)(2,1)S(1)}) custom-call(bf16[528,256]{1,0:T(8,128)(2,1)S(1)} %fusion.2.kv_hbm, bf16[6,256,256]{2,1,0:T(8,128)(2,1)S(1)} %bitcast_dynamic-update-slice_fusion.qt_ref, bf16[256,2048]{1,0:T(8,128)(2,1)S(1)} %copy-done, ...), custom_call_target="tpu_custom_call" | custom-call | tf_op jit(solution)/shard_map/attend/pallas_call | solution.py:303
  105.6 0.7 copy-done.2
  106.3 0.7 copy-done.3
  107.0 0.1 slice_reduce_fusion
  107.1 0.1 eq.109
  107.2 0.1 compare_reduce_fusion
  107.3 0.1 convolution_bitcast_fusion
  107.4 0.1 fusion.24
  107.5 0.1 and.179
  107.6 0.2 and.180
  107.9 0.1 and.181
  108.0 0.1 and.182
  108.1 0.7 and_convert_fusion.sel_ref
  108.8 0.1 pad_add_fusion
  108.9 0.8 fusion.1.pick_ref
  109.7 0.1 copy.69
  109.8 0.7 broadcast_divide_fusion.share_ref
  110.5 0.7 fusion.31.perm_ref
  111.2 128.4 %experts.1 = bf16[64,2048]{1,0:T(8,128)(2,1)} custom-call(bf16[64,2048]{1,0:T(8,128)(2,1)} %copy-done.3, bf16[64,2048]{1,0:T(8,128)(2,1)} %copy-done.2, bf16[8,32,256]{2,1,0:T(8,128)(2,1)} %and_convert_fusion.sel_ref, bf16[64,64]{1,0:T(8,128)(2,1)} %fusion.31.perm_ref, bf16[256,512]{1,0:T(8,128)(2,1)} %fusion.1.pick_ref, ...), custom_call_target="tpu_custom_call" | custom-call | tf_op jit(solution)/shard_map/experts/pallas_call | solution.py:727
  239.6 1.7 copy.82
  (51 shorter events, 0.5 us)
Async XLA Ops:
  0.0 2.7 %copy-start.7 = (bf16[256,256]{1,0:T(8,128)(2,1)S(1)}, bf16[256,256]{1,0:T(8,128)(2,1)}, u32[]{:S(2)}) copy-start(bf16[256,256]{1,0:T(8,128)(2,1)} %param.19) | copy-start | bytes 393220
  0.0 2.9 %copy-start.11 = (f32[64]{0:T(128)S(1)}, f32[64]{0:T(128)}, u32[]{:S(2)}) copy-start(f32[64]{0:T(128)} %param.25) | copy-start | bytes 772
  0.0 0.5 copy-start.10
  2.4 0.9 copy-start.8
  2.4 1.0 copy-start.12
  2.7 1.0 copy-start.6
  2.7 1.1 copy-start.13
  3.1 8.0 %copy-start = (bf16[256,2048]{1,0:T(8,128)(2,1)S(1)}, bf16[256,2048]{1,0:T(8,128)(2,1)}, u32[]{:S(2)}) copy-start(bf16[256,2048]{1,0:T(8,128)(2,1)} %ws_hbm.1) | copy-start | bytes 3145732
  3.2 8.0 %copy-start.1 = (bf16[256,2048]{1,0:T(8,128)(2,1)S(1)}, bf16[256,2048]{1,0:T(8,128)(2,1)}, u32[]{:S(2)}) copy-start(bf16[256,2048]{1,0:T(8,128)(2,1)} %wl_hbm.1) | copy-start | bytes 3145732
  3.2 8.0 %copy-start.4 = (bf16[64,2048]{1,0:T(8,128)(2,1)S(1)}, bf16[64,2048]{1,0:T(8,128)(2,1)}, u32[]{:S(2)}) copy-start(bf16[64,2048]{1,0:T(8,128)(2,1)} %res_ref.1) | copy-start | bytes 786436
  3.2 8.0 %copy-start.5 = (f32[2048]{0:T(1024)S(1)}, f32[2048]{0:T(1024)}, u32[]{:S(2)}) copy-start(f32[2048]{0:T(1024)} %param.32) | copy-start | bytes 24580
  11.2 98.5 %copy-start.9 = (f32[64,2]{0,1:T(2,128)S(1)}, f32[64,2]{0,1:T(2,128)}, u32[]{:S(2)}) copy-start(f32[64,2]{0,1:T(2,128)} %param.34) | copy-start | bytes 1540
  105.6 0.7 copy-start.2
  106.3 0.7 copy-start.3

commit v4 on v0

v4 whole, which is shorter than its diff:
```python
import functools
import jax
import jax.numpy as jnp
import numpy as np
from jax import lax
from jax.experimental import pallas as pl
from jax.experimental.pallas import tpu as pltpu
from jax.sharding import PartitionSpec as P

HS_SMALL = 64
HS_LARGE = 128
GRID_W = 64
LANES = 128
LOG2E = 1.4426950408889634
theta_base = 10000.0
norm_eps = 1e-06
SEATS = 4
MESH = pl.DeviceIdType.MESH
BF16 = jnp.bfloat16
F32 = jnp.float32


def _send(src, dst, ssem, rsem, axis, dev):
    return pltpu.make_async_remote_copy(
        src_ref=src,
        dst_ref=dst,
        send_sem=ssem,
        recv_sem=rsem,
        device_id={axis: dev},
        device_id_type=MESH,
    )


def _iota(shape, dim):
    return lax.broadcasted_iota(jnp.int32, shape, dim)


class Ring:
    def __init__(self, buf, parts, ssem, rsem, psem, right, left, partner, last):
        self.buf, self.parts, self.last = buf, parts, last
        self.ssem, self.rsem, self.psem = ssem, rsem, psem
        self.right, self.left, self.partner = right, left, partner

    def at(self, pair, side, part):
        return self.buf.at[pair, side, self.parts[part]]

    def to_right(self, step, pair, part, dst_pair):
        return _send(
            self.at(pair, 0, part),
            self.at(dst_pair, 0, part),
            self.ssem.at[step, 0, part],
            self.rsem.at[dst_pair, 0, part],
            "sp",
            self.right,
        )

    def to_left(self, step, pair, part, dst_pair, src_side=1, dst_side=1):
        return _send(
            self.at(pair, src_side, part),
            self.at(dst_pair, dst_side, part),
            self.ssem.at[step, 1, part],
            self.rsem.at[dst_pair, dst_side, part],
            "sp",
            self.left,
        )

    def to_partner(self, pair, side, part, dst_pair, dst_side):
        return _send(
            self.at(pair, side, part),
            self.at(dst_pair, dst_side, part),
            self.psem.at[dst_pair, dst_side, part],
            self.rsem.at[dst_pair, dst_side, part],
            "sp",
            self.partner,
        )

    def arrived(self, pair, side, part):
        self.to_partner(pair, side, part, pair, side).wait_recv()

    def first(self, part):
        return (
            self.to_right(1, 0, part, 1),
            self.to_left(1, 0, part, 1, src_side=0),
            self.to_partner(0, 0, part, 0, 1),
        )

    def begin(self, part):
        for copy in self.first(part):
            copy.start()

    def pass_on(self, step, part):
        pair, last = 2 * step - 1, self.last
        for side in range(2):
            self.arrived(pair, side, part)

        @pl.when(step < last - 1)
        def _():
            self.to_right(step + 1, pair, part, pair + 2).start()
            self.to_left(step + 1, pair, part, pair + 2).start()

        @pl.when(step == last - 1)
        def _():
            if part == 0:
                self.to_right(step + 1, pair, 0, 2 * last - 1).start()
            else:
                self.to_left(step + 1, pair, 1, 2 * last - 1, dst_side=0).start()

        for side in range(2):
            self.to_partner(pair, side, part, pair + 1, side).start()

    def opposite(self):
        pair = 2 * self.last - 1
        for part in range(2):
            self.arrived(pair, 0, part)
            self.to_partner(pair, 0, part, pair, 1).start()

    def opposite_partner(self):
        for part in range(2):
            self.arrived(2 * self.last - 1, 1, part)

    def finish(self):
        last = self.last
        for part in range(2):
            for copy in self.first(part):
                copy.wait_send()

        def sent(step, carry):
            pair = 2 * step - 1
            for part in range(2):

                @pl.when(step < last - 1)
                def _():
                    self.to_right(step + 1, pair, part, pair + 2).wait_send()
                    self.to_left(step + 1, pair, part, pair + 2).wait_send()

                for side in range(2):
                    self.to_partner(pair, side, part, pair + 1, side).wait_send()
            return carry

        lax.fori_loop(1, last, sent, 0)
        self.to_right(last, 2 * last - 3, 0, 2 * last - 1).wait_send()
        self.to_left(last, 2 * last - 3, 1, 2 * last - 1, dst_side=0).wait_send()
        for part in range(2):
            self.to_partner(2 * last - 1, 0, part, 2 * last - 1, 1).wait_send()


def layer_kernel(
    heads,
    qs_ref,
    ks_ref,
    vs_ref,
    ql_ref,
    kl_ref,
    vl_ref,
    gqs_ref,
    gks_ref,
    gql_ref,
    gkl_ref,
    col_hbm,
    row_hbm,
    ws_hbm,
    wl_hbm,
    res_ref,
    gain_ref,
    names_ref,
    score_ref,
    wg_hbm,
    wu_hbm,
    wd_hbm,
    out_ref,
    kvbuf,
    qt,
    coltab,
    rowtab,
    tabs,
    wbuf,
    acc,
    mbuf,
    lbuf,
    hbuf,
    cbuf,
    dbuf,
    abuf,
    xbuf,
    wg,
    wu,
    wd,
    gbuf,
    pbuf,
    rbuf,
    fbuf,
    obuf,
    ret,
    below,
    perm,
    pick,
    lsem,
    rsem,
    ssem,
    psem,
    xr,
    xs,
    rsem2,
    ssem2,
    psem2,
    gr,
    gs,
    rr,
    rs,
    tr,
    ts,
):
    n_sp = lax.axis_size("sp")
    n_z = n_sp // 2
    last = n_z // 2
    tok = kvbuf.shape[3]
    kv_rows = kvbuf.shape[2]
    rows, width = res_ref.shape
    sp = lax.axis_index("sp")
    tp = lax.axis_index("tp")
    z = sp // 2
    core = lax.rem(sp, 2)
    right = lax.rem(sp + 2, n_sp)
    left = lax.rem(sp + n_sp - 2, n_sp)
    partner = sp + 1 - 2 * core
    x_right = lax.rem(tp + 1, 4)
    x_left = lax.rem(tp + 3, 4)
    x_far = lax.rem(tp + 2, 4)
    grid_rows = tok // GRID_W

    loads = [
        pltpu.make_async_copy(a, b, lsem.at[i])
        for i, (a, b) in enumerate(
            (
                (col_hbm, coltab),
                (row_hbm.at[pl.ds(sp * grid_rows, grid_rows)], rowtab),
                (ws_hbm, wbuf.at[pl.ds(0, ws_hbm.shape[0])]),
                (wl_hbm, wbuf.at[pl.ds(ws_hbm.shape[0], wl_hbm.shape[0])]),
                (wg_hbm, wg),
                (wu_hbm, wu),
                (wd_hbm, wd),
            )
        )
    ]
    loads[0].start()
    loads[1].start()

    barrier = pltpu.get_barrier_semaphore()

    def greet(i, carry):
        pl.semaphore_signal(
            barrier, inc=1, device_id={"sp": lax.rem(sp + i, n_sp)}, device_id_type=MESH
        )
        return carry

    lax.fori_loop(1, n_sp, greet, 0)
    for dev in (x_right, x_left):
        pl.semaphore_signal(barrier, inc=1, device_id={"tp": dev}, device_id_type=MESH)

    ring = Ring(
        kvbuf,
        (pl.ds(0, tok), pl.ds(tok, kv_rows - tok)),
        ssem,
        rsem,
        psem,
        right,
        left,
        partner,
        last,
    )
    tokens = Ring(
        xbuf,
        (pl.ds(0, rows // 2), pl.ds(rows // 2, rows // 2)),
        ssem2,
        rsem2,
        psem2,
        right,
        left,
        partner,
        last,
    )

    lane = _iota((tok, LANES), 1)

    def turned(raw, gain, table, size):
        x = raw.astype(F32)
        square = x * x
        if size < LANES:
            lower = lane < size
            mean = jnp.where(
                lower,
                jnp.sum(jnp.where(lower, square, 0.0), axis=1, keepdims=True),
                jnp.sum(jnp.where(lower, 0.0, square), axis=1, keepdims=True),
            ) * (1.0 / size)
            gain = jnp.concatenate([gain, gain], axis=1)
        else:
            mean = jnp.sum(square, axis=1, keepdims=True) * (1.0 / size)
        x = x * lax.rsqrt(mean + norm_eps) * gain
        quarter = size // 4
        swapped = jnp.where(
            lane % (2 * quarter) < quarter,
            pltpu.roll(x, LANES - quarter, 1),
            pltpu.roll(x, quarter, 1),
        )
        return x * tabs[table] + swapped * tabs[table + 1]

    kvbuf[0, 0, pl.ds(tok, LANES), :] = jnp.transpose(vs_ref[...].astype(F32)).astype(BF16)
    kvbuf[0, 0, pl.ds(tok + LANES, LANES), :] = jnp.transpose(vl_ref[...].astype(F32)).astype(BF16)
    names = names_ref[...].astype(F32)
    repeat = (_iota((16, 2), 0) % 2 == _iota((16, 2), 1)).astype(BF16)
    named = jnp.dot(repeat, names.astype(BF16), preferred_element_type=F32).astype(BF16)
    spread = (_iota((rows, tok), 1) % rows == _iota((rows, tok), 0)).astype(BF16)
    named = jnp.dot(named, spread, preferred_element_type=F32)
    own_lane = _iota((16, tok), 1) // rows == _iota((16, tok), 0) // 2
    kvbuf[0, 0, pl.ds(2 * tok, 16), :] = jnp.where(own_lane, named, 0.0).astype(BF16)

    loads[0].wait()
    loads[1].wait()
    for i in range(4):
        for g in range(grid_rows):
            tabs[i, pl.ds(g * GRID_W, GRID_W), :] = coltab[i] + rowtab[g, pl.ds(i, 1), :]
    kvbuf[0, 0, pl.ds(0, tok), pl.ds(0, LANES)] = turned(
        ks_ref[...], gks_ref[...], 0, HS_SMALL
    ).astype(BF16)
    kvbuf[0, 0, pl.ds(0, tok), pl.ds(LANES, LANES)] = turned(
        kl_ref[...], gkl_ref[...], 2, HS_LARGE
    ).astype(BF16)

    pl.semaphore_wait(barrier, n_sp + 1)
    for part in range(2):
        ring.begin(part)
    for load in loads[2:]:
        load.start()

    qt[...] = jnp.zeros_like(qt)
    h = 0
    for ref, gain_of, table, size, base in (
        (qs_ref, gqs_ref, 0, HS_SMALL, 0),
        (ql_ref, gql_ref, 2, HS_LARGE, LANES),
    ):
        for i in range(ref.shape[1] // LANES):
            flipped = jnp.transpose(
                turned(ref[:, pl.ds(i * LANES, LANES)], gain_of[...], table, size)
            ).astype(BF16)
            for j in range(LANES // size):
                at = base + (h - base // LANES * 4) // 2 * size
                qt[h, pl.ds(at, size), :] = flipped[j * size : (j + 1) * size]
                h += 1

    acc[...] = jnp.zeros_like(acc)
    lbuf[...] = jnp.zeros_like(lbuf)
    mbuf[...] = jnp.full(mbuf.shape, -1e30, F32)

    below[...] = (
        (_iota((tok, tok), 0) < _iota((tok, tok), 1))
        & (_iota((tok, tok), 0) // rows == _iota((tok, tok), 1) // rows)
    ).astype(BF16)
    out_row = _iota((64, 64), 0)
    in_row = (
        (out_row // 8) % 2 * 32 + (out_row % 8) // SEATS * 16 + out_row // 16 * SEATS
    ) + out_row % SEATS
    perm[...] = (in_row == _iota((64, 64), 1)).astype(BF16)
    eye = (_iota((rows, rows), 0) == _iota((rows, rows), 1)).astype(BF16)
    columns = lax.dot_general(
        eye, names.astype(BF16), (((1,), (1,)), ((), ())), preferred_element_type=F32
    )
    earlier = _iota((rows, rows), 1) < _iota((rows, rows), 0)
    for k in range(2):
        column = columns[:, k : k + 1]
        same = ((column == names[0:1, :]) | (column == names[1:2, :])) & earlier
        rank = jnp.sum(same.astype(F32), axis=1, keepdims=True).astype(jnp.int32)
        expert = column.astype(jnp.int32)
        host = expert // 2
        away = z - host // 2
        away = jnp.where(away < 0, away + n_z, away)
        other = (host % 2 != core).astype(jnp.int32)
        step = jnp.minimum(away, n_z - away)
        edge = (away == 0) | (away == last)
        pair = jnp.where(
            away == 0, 0, jnp.where(away == last, 2 * last - 1, 2 * step - 1 + other)
        )
        side = jnp.where(edge, other, (away < last).astype(jnp.int32))
        base = (pair * 2 + side) * 16 + expert % 2 * SEATS + rank
        seat = _iota((rows, pick.shape[1]), 1)
        pick[pl.ds(k * rows, rows), :] = (seat == base).astype(BF16)
        pick[pl.ds((2 + k) * rows, rows), :] = (seat == base + 8).astype(BF16)

    def attend(pair):
        keys = kvbuf[pair, :, pl.ds(0, tok), :].reshape(2 * tok, tok)
        for h, (a0, size, v0, scale) in enumerate(heads):
            s = jnp.dot(keys, qt[h], preferred_element_type=F32)
            m_old = mbuf[h]
            m_new = jnp.maximum(m_old, jnp.max(s, axis=0, keepdims=True))
            p = jnp.exp2((s - m_new) * (scale * LOG2E))
            shrink = jnp.exp2((m_old - m_new) * (scale * LOG2E))
            mbuf[h] = m_new
            lbuf[h] = lbuf[h] * shrink + jnp.sum(p, axis=0, keepdims=True)
            pb = p.astype(BF16)
            pv = jnp.dot(
                kvbuf[pair, 0, pl.ds(tok + v0, size), :],
                pb[:tok],
                preferred_element_type=F32,
            ) + jnp.dot(
                kvbuf[pair, 1, pl.ds(tok + v0, size), :],
                pb[tok:],
                preferred_element_type=F32,
            )
            acc[pl.ds(a0, size), :] = acc[pl.ds(a0, size), :] * shrink + pv

    def attend_turn(t, carry):
        step = t // 2 + 1
        phase = lax.rem(t, 2)
        for part in range(2):

            @pl.when((phase == part) & (step < last))
            def _():
                ring.pass_on(step, part)

        @pl.when(t == 0)
        def _():
            for part in range(2):
                ring.arrived(0, 1, part)

        @pl.when((phase == 0) & (t > 0))
        def _():
            for side in range(2):
                for part in range(2):
                    ring.arrived(t, side, part)

        @pl.when(t == 2 * last - 1)
        def _():
            ring.opposite()
            ring.opposite_partner()

        attend(t)
        return carry

    lax.fori_loop(0, 2 * last, attend_turn, 0)

    loads[2].wait()
    loads[3].wait()
    for h, (a0, size, v0, scale) in enumerate(heads):
        acc[pl.ds(a0, size), :] = acc[pl.ds(a0, size), :] / lbuf[h]
    heard = jnp.transpose(acc[...]).astype(BF16)
    hbuf[...] = heard.reshape(4, rows, heard.shape[1])

    def project(where, owner):
        cbuf[where] = jnp.dot(hbuf[owner], wbuf[...], preferred_element_type=F32).astype(BF16)

    lo, hi = pl.ds(0, rows // 2), pl.ds(rows // 2, rows // 2)
    project(0, x_far)
    first_r = _send(cbuf.at[0, lo], dbuf.at[3, lo], xs.at[0], xr.at[0], "tp", x_right)
    first_l = _send(cbuf.at[0, hi], dbuf.at[3, hi], xs.at[1], xr.at[1], "tp", x_left)
    first_r.start()
    first_l.start()
    project(1, x_right)
    near_r = _send(cbuf.at[1], dbuf.at[0], xs.at[2], xr.at[2], "tp", x_right)
    near_r.start()
    project(2, x_left)
    near_l = _send(cbuf.at[2], dbuf.at[1], xs.at[3], xr.at[3], "tp", x_left)
    near_l.start()
    project(3, tp)
    first_r.wait_recv()
    pass_r = _send(dbuf.at[3, lo], dbuf.at[2, lo], xs.at[4], xr.at[4], "tp", x_right)
    pass_r.start()
    first_l.wait_recv()
    pass_l = _send(dbuf.at[3, hi], dbuf.at[2, hi], xs.at[5], xr.at[5], "tp", x_left)
    pass_l.start()
    ring.finish()
    near_r.wait_recv()
    near_l.wait_recv()
    pass_r.wait_recv()
    pass_l.wait_recv()
    for part, half in enumerate((lo, hi)):
        total = (
            cbuf[3, half].astype(F32)
            + dbuf[0, half].astype(F32)
            + dbuf[1, half].astype(F32)
            + dbuf[2, half].astype(F32)
        )
        attended = (res_ref[half].astype(F32) + total).astype(BF16)
        abuf[half] = attended
        wide = attended.astype(F32)
        xbuf[0, 0, half] = (
            wide
            * lax.rsqrt(jnp.mean(wide * wide, axis=-1, keepdims=True) + norm_eps)
            * gain_ref[...]
        ).astype(BF16)
        tokens.begin(part)
    for c in (first_r, first_l, near_r, near_l, pass_r, pass_l):
        c.wait_send()

    def share_right(c):
        return _send(gbuf.at[c, 0], gbuf.at[c, 1], gs.at[c, 0], gr.at[c, 0], "tp", x_right)

    def share_left(c):
        return _send(gbuf.at[c, 0], gbuf.at[c, 2], gs.at[c, 1], gr.at[c, 1], "tp", x_left)

    def pass_right(c):
        return _send(
            gbuf.at[c, 1, 0], gbuf.at[c, 3, 0], gs.at[c, 2], gr.at[c, 2], "tp", x_right
        )

    def pass_left(c):
        return _send(gbuf.at[c, 2, 1], gbuf.at[c, 3, 1], gs.at[c, 3], gr.at[c, 3], "tp", x_left)

    def far_right(c):
        return _send(pbuf.at[c, 3, 0], rbuf.at[c, 0], rs.at[c, 0], rr.at[c, 0], "tp", x_right)

    def far_left(c):
        return _send(pbuf.at[c, 3, 1], rbuf.at[c, 1], rs.at[c, 1], rr.at[c, 1], "tp", x_left)

    def near_right(c):
        return _send(pbuf.at[c, 2], fbuf.at[c, 0], rs.at[c, 2], rr.at[c, 2], "tp", x_right)

    def near_left(c):
        return _send(pbuf.at[c, 1], fbuf.at[c, 1], rs.at[c, 3], rr.at[c, 3], "tp", x_left)

    def seats_of(c):
        row = _iota((16, tok), 0)
        kept = jnp.zeros((16, tok), F32)
        for q in range(4):
            block = kvbuf[2 * c + q // 2, q % 2, pl.ds(2 * tok, 16), :].astype(F32)
            kept = jnp.where(row // 2 == q, block, kept)
        name0 = jnp.sum(jnp.where(row % 2 == 0, kept, 0.0), axis=0, keepdims=True)
        name1 = jnp.sum(jnp.where(row % 2 == 1, kept, 0.0), axis=0, keepdims=True)
        wide_row = _iota((32, tok), 0)
        mine = (2 * sp + wide_row // 16).astype(F32)
        member = (name0 == mine) | (name1 == mine)
        rank = jnp.dot(member.astype(F32).astype(BF16), below[...], preferred_element_type=F32)
        seated = (
            member
            & (rank == (wide_row % SEATS).astype(F32))
            & (_iota((32, tok), 1) // rows == wide_row % 16 // SEATS)
        )
        return seated.astype(F32).astype(BF16)

    def run_experts(c):
        for e in range(2):
            x = gbuf[c, :, e].reshape(64, width)
            gate = jnp.dot(x, wg[e], preferred_element_type=F32)
            up = jnp.dot(x, wu[e], preferred_element_type=F32)
            active = (gate / (1.0 + jnp.exp(-gate)) * up).astype(BF16)
            term = jnp.dot(active, wd[e], preferred_element_type=F32)
            pbuf[c, :, e] = term.astype(BF16).reshape(4, 16, width)

    def gather_turn(c):
        step = c + 1

        @pl.when(step < last)
        def _():
            for part in range(2):
                tokens.pass_on(step, part)

        @pl.when(step == last)
        def _():
            tokens.opposite()

        @pl.when(c == 0)
        def _():
            for part in range(2):
                tokens.arrived(0, 1, part)

        @pl.when((c > 0) & (c < last))
        def _():
            for side in range(2):
                for part in range(2):
                    tokens.arrived(2 * c, side, part)

        @pl.when(step == last)
        def _():
            tokens.opposite_partner()

        @pl.when(c < last)
        def _():
            block = xbuf[pl.ds(2 * c, 2)].reshape(4 * rows, width)
            chosen = jnp.dot(seats_of(c), block, preferred_element_type=F32)
            gbuf[c, 0] = chosen.astype(BF16).reshape(2, 16, width)
            share_right(c).start()
            share_left(c).start()

        @pl.when((c >= 1) & (c < last + 1))
        def _():
            share_right(c - 1).wait_recv()
            pass_right(c - 1).start()
            share_left(c - 1).wait_recv()
            pass_left(c - 1).start()

        @pl.when(c == 2)
        def _():
            for load in loads[4:]:
                load.wait()

        @pl.when((c >= 2) & (c < last + 2))
        def _():
            pass_right(c - 2).wait_recv()
            pass_left(c - 2).wait_recv()
            run_experts(c - 2)

    def home(c, q):
        if q == 0:
            return lax.rem(z - c + n_z, n_z) * 2 + 1 - core, 2 * c, 0
        if q == 1:
            return lax.rem(z + c, n_z) * 2 + 1 - core, 2 * c, 1
        if q == 2:
            return lax.rem(z - c - 1 + n_z, n_z) * 2 + core, 2 * c + 1, 0
        return lax.rem(z + c + 1, n_z) * 2 + core, 2 * c + 1, 1

    def give(c, q):
        dev, pair, side = home(c, q)
        return _send(
            obuf.at[c, q], ret.at[pair, side], ts.at[c, q], tr.at[pair, side], "sp", dev
        )

    def give_last():
        dev = lax.rem(z + last, n_z) * 2 + 1 - core
        return _send(
            obuf.at[last - 1, 3],
            ret.at[2 * last - 1, 1],
            ts.at[last - 1, 3],
            tr.at[2 * last - 1, 1],
            "sp",
            dev,
        )

    def order(i):
        half = last // 2
        late = i // half
        return (1 - late) * (i + half) + late * (last - 1 - i)

    def return_turn(i):
        @pl.when((i >= 1) & (i < last + 1))
        def _():
            c = order(i - 1)
            far_right(c).wait_recv()
            pbuf[c, 2, 0] = (pbuf[c, 2, 0].astype(F32) + rbuf[c, 0].astype(F32)).astype(BF16)
            near_right(c).start()
            far_left(c).wait_recv()
            pbuf[c, 1, 1] = (pbuf[c, 1, 1].astype(F32) + rbuf[c, 1].astype(F32)).astype(BF16)
            near_left(c).start()

        @pl.when((i >= 0) & (i < last))
        def _():
            c = order(i)
            far_right(c).start()
            far_left(c).start()

        @pl.when(i >= 2)
        def _():
            c = order(i - 2)
            near_right(c).wait_recv()
            near_left(c).wait_recv()
            total = pbuf[c, 0].astype(F32) + fbuf[c, 0].astype(F32) + fbuf[c, 1].astype(F32)
            total = total.astype(BF16).reshape(32, width)
            split = jnp.concatenate([total[:, : width // 2], total[:, width // 2 :]], axis=0)
            ordered = jnp.dot(perm[...], split, preferred_element_type=F32)
            obuf[c] = ordered.astype(BF16).reshape(4, 16, width // 2)

            @pl.when(c > 0)
            def _():
                give(c, 0).start()

            @pl.when(c == 0)
            def _():
                ret[0, 0] = obuf[0, 0]

            give(c, 1).start()
            give(c, 2).start()

            @pl.when(c < last - 1)
            def _():
                give(c, 3).start()

            @pl.when(c == last - 1)
            def _():
                give_last().start()

    def turn(t, carry):
        gather_turn(t)
        return_turn(t - (last - 1))
        return carry

    lax.fori_loop(0, 2 * last + 1, turn, 0)

    tokens.finish()

    def left_all(c, carry):
        for copy in (share_right, share_left, pass_right, pass_left):
            copy(c).wait_send()
        for copy in (far_right, far_left, near_right, near_left):
            copy(c).wait_send()
        return carry

    lax.fori_loop(0, last, left_all, 0)

    def came(c, carry):
        @pl.when(c > 0)
        def _():
            give(c, 0).wait_recv()

        for q in (1, 2, 3):
            give(c, q).wait_recv()
        return carry

    lax.fori_loop(0, last, came, 0)

    back = ret[...].reshape(ret.shape[0] * 32, width // 2)
    picked = jnp.dot(pick[...], back, preferred_element_type=F32)
    scores = score_ref[...]
    scores = scores / (scores[:, 0:1] + scores[:, 1:2])
    one, two = scores[:, 0:1], scores[:, 1:2]
    out = abuf[...].astype(F32)
    lower = picked[:rows] * one + picked[rows : 2 * rows] * two
    upper = picked[2 * rows : 3 * rows] * one + picked[3 * rows :] * two
    out_ref[:, : width // 2] = (out[:, : width // 2] + lower).astype(BF16)
    out_ref[:, width // 2 :] = (out[:, width // 2 :] + upper).astype(BF16)

    def gone(c, carry):
        @pl.when(c > 0)
        def _():
            give(c, 0).wait_send()

        for q in (1, 2, 3):
            give(c, q).wait_send()
        return carry

    lax.fori_loop(0, last, gone, 0)


def turn_tables(places, size, by_row):
    lane = np.arange(LANES) % size
    quarter = size // 4
    rates = np.power(
        np.float32(theta_base), (-2.0 * np.arange(quarter) / (size // 2)).astype(np.float32)
    ).astype(np.float32)
    angles = (places[:, None].astype(np.float32) * rates[lane % quarter]).astype(np.float32)
    here = (lane < size // 2) if by_row else (lane >= size // 2)
    sign = np.where(lane % (2 * quarter) < quarter, -1.0, 1.0)
    cosine = np.where(here, np.cos(angles), 0.0)
    sine = np.where(here, np.sin(angles) * sign, 0.0)
    return cosine.astype(np.float32), sine.astype(np.float32)


def on_device(
    queries_small,
    keys_small,
    values_small,
    queries_large,
    keys_large,
    values_large,
    query_gain_small,
    key_gain_small,
    query_gain_large,
    key_gain_large,
    residual_in,
    out_weight_small,
    out_weight_large,
    norm_gain,
    routes,
    route_scores,
    expert_gate,
    expert_up,
    expert_down,
):
    tok = queries_small.shape[0]
    rows, width = residual_in.shape
    n_sp = lax.axis_size("sp")
    pairs = n_sp // 2
    chunks = pairs // 2
    depth = out_weight_small.shape[0] + out_weight_large.shape[0]
    kv_rows = 2 * tok + 16
    grid_rows = tok // GRID_W
    row_places = np.arange(n_sp * grid_rows)
    col_places = np.arange(GRID_W)
    row_tables, col_tables = [], []
    for size in (HS_SMALL, HS_LARGE):
        row_tables.extend(turn_tables(row_places, size, True))
        col_tables.extend(turn_tables(col_places, size, False))
    heads = []
    wide_small = keys_small.shape[1]
    for count, kv_count, size, a0, v0 in (
        (queries_small.shape[1] // HS_SMALL, wide_small // HS_SMALL, HS_SMALL, 0, 0),
        (
            queries_large.shape[1] // HS_LARGE,
            keys_large.shape[1] // HS_LARGE,
            HS_LARGE,
            queries_small.shape[1],
            wide_small,
        ),
    ):
        for h in range(count):
            kv = h // (count // kv_count)
            heads.append((a0 + h * size, size, v0 + kv * size, size ** (-0.5)))
    vmem = pl.BlockSpec(memory_space=pltpu.VMEM)
    hbm = pl.BlockSpec(memory_space=pl.ANY)
    dma = pltpu.SemaphoreType.DMA
    V = pltpu.VMEM
    return pl.pallas_call(
        functools.partial(layer_kernel, tuple(heads)),
        out_shape=jax.ShapeDtypeStruct((rows, width), BF16),
        in_specs=[vmem] * 10 + [hbm] * 4 + [vmem] * 4 + [hbm] * 3,
        out_specs=vmem,
        scratch_shapes=[
            V((pairs, 2, kv_rows, tok), BF16),
            V((len(heads), tok, tok), BF16),
            V((4, GRID_W, LANES), F32),
            V((grid_rows, 4, LANES), F32),
            V((4, tok, LANES), F32),
            V((depth, width), BF16),
            V((depth, tok), F32),
            V((len(heads), 1, tok), F32),
            V((len(heads), 1, tok), F32),
            V((4, rows, depth), BF16),
            V((4, rows, width), BF16),
            V((4, rows, width), BF16),
            V((rows, width), BF16),
            V((pairs, 2, rows, width), BF16),
            V(expert_gate.shape, BF16),
            V(expert_up.shape, BF16),
            V(expert_down.shape, BF16),
            V((chunks, 4, 2, 16, width), BF16),
            V((chunks, 4, 2, 16, width), BF16),
            V((chunks, 2, 16, width), BF16),
            V((chunks, 2, 2, 16, width), BF16),
            V((chunks, 4, 16, width // 2), BF16),
            V((pairs, 2, 16, width // 2), BF16),
            V((tok, tok), BF16),
            V((64, 64), BF16),
            V((4 * rows, pairs * 32), BF16),
            dma((7,)),
            dma((pairs, 2, 2)),
            dma((chunks + 1, 2, 2)),
            dma((pairs, 2, 2)),
            dma((6,)),
            dma((6,)),
            dma((pairs, 2, 2)),
            dma((chunks + 1, 2, 2)),
            dma((pairs, 2, 2)),
            dma((chunks, 4)),
            dma((chunks, 4)),
            dma((chunks, 4)),
            dma((chunks, 4)),
            dma((pairs, 2)),
            dma((chunks, 4)),
        ],
        compiler_params=pltpu.CompilerParams(
            collective_id=0, has_side_effects=True, vmem_limit_bytes=58 * 1024 * 1024
        ),
        name="layer",
    )(
        queries_small,
        keys_small,
        values_small,
        queries_large,
        keys_large,
        values_large,
        query_gain_small.reshape(1, -1),
        key_gain_small.reshape(1, -1),
        query_gain_large.reshape(1, -1),
        key_gain_large.reshape(1, -1),
        jnp.asarray(np.stack(col_tables)),
        jnp.asarray(np.stack(row_tables, axis=1)),
        out_weight_small,
        out_weight_large,
        residual_in,
        norm_gain.reshape(1, -1),
        routes.T,
        route_scores,
        expert_gate,
        expert_up,
        expert_down,
    )


def solution(mesh):
    in_specs = (
        P(("grp", "sp"), "tp"),
        P(("grp", "sp"), "tp"),
        P(("grp", "sp"), "tp"),
        P(("grp", "sp"), "tp"),
        P(("grp", "sp"), "tp"),
        P(("grp", "sp"), "tp"),
        P("grp"),
        P("grp"),
        P("grp"),
        P("grp"),
        P(("grp", "sp", "tp"), None),
        P("tp", None),
        P("tp", None),
        P(),
        P(("grp", "sp", "tp"), None),
        P(("grp", "sp", "tp"), None),
        P("sp", None, "tp"),
        P("sp", None, "tp"),
        P("sp", "tp", None),
    )
    out_specs = P(("grp", "sp", "tp"), None)
    return jax.shard_map(
        on_device, mesh=mesh, in_specs=in_specs, out_specs=out_specs, check_vma=False
    )
```

time: 522 us -> 215 us (0.41)
  waiting for transfers between devices: 274 us -> 0 us
  Pallas kernels: 0 us -> 212 us
  matrix products: 86.1 us -> 0 us
  blocking collectives: 64.4 us -> 0 us
  other arithmetic: 33.7 us -> 0 us
  local copies, waits for them, and re-layouts: 30 us -> 3.05 us
  starting transfers between devices: 17.5 us -> 0 us
  between operations: 13.6 us -> 0.01 us
    pallas_call x0 -> x1, Pallas kernels: none -> 212 us  [on_device(): pl.pallas_call(functools.partial(layer_kernel, tuple(heads)), out_shape=j...]
    all_gather x2 -> x0, waiting for transfers between devices: 152 us -> none  [the longest x1 108 us: sent_together(): lax.all_gather(both, axis, axis=dim, tiled=True)]
    dot_general x38 -> x0, matrix products: 86.1 us -> none  [the longest x16 43.6 us: attend_block(): jnp.einsum('qgrd,kgd->qgrk', queries, key_heads, preferred_element_type=j...]
    all_to_all x2 -> x0, waiting for transfers between devices: 69.1 us -> none  [the longest x1 55.4 us: on_device(): lax.all_to_all(summed, 'sp', split_axis=0, concat_axis=0, tiled=True)]
    all_to_all x1 -> x0, blocking collectives: 64.4 us -> none  [on_device(): lax.all_to_all(outgoing, 'sp', split_axis=0, concat_axis=0, tiled=True)]
    reduce_scatter x1 -> x0, waiting for transfers between devices: 53.5 us -> none  [on_device(): lax.psum_scatter(jnp.einsum('secf,efd->secd', active, expert_down, prefer...]
    reduce_sum x25 -> x0, other arithmetic: 29 us -> none  [the longest x16 27.2 us: attend_block(): weight_sum = weight_sum * shrink + jnp.sum(weights, axis=-1)]
    all_to_all x2 -> x0, starting transfers between devices: 17.3 us -> none  [the longest x1 13.2 us: on_device(): lax.all_to_all(summed, 'sp', split_axis=0, concat_axis=0, tiled=True)]
  transfers between devices with their start and end apart: 5 -> 0, of which waited for: 5 -> 0; matrix products, arithmetic and copies ran while one was open for 0% -> 0% of each run, Pallas kernels for 0% -> 0%
where the time goes in v4:
time: 215 us
  Pallas kernels  212 us (99%)
  local copies, waits for them, and re-layouts  3.05 us (1%)
    pallas_call x1, Pallas kernels, on_device(): pl.pallas_call(functools.partial(layer_kernel, tuple(heads)), out_shape=j...  212 us

profile of v4, /device:TPU:33, one launch (start us, length us, event | category | flops | bytes accessed | tf_op | source)
XLA Modules:
  0.0 214.9 jit_solution(13814594084884207297)
XLA Ops:
  0.0 1.4 copy.22.score_ref
  1.4 211.9 %layer.1 = bf16[64,2048]{1,0:T(8,128)(2,1)} custom-call(bf16[256,256]{1,0:T(8,128)(2,1)} %qs_ref.1, bf16[256,128]{1,0:T(8,128)(2,1)} %ks_ref.1, bf16[256,128]{1,0:T(8,128)(2,1)} %vs_ref.1, bf16[256,256]{1,0:T(8,128)(2,1)} %ql_ref.1, bf16[256,128]{1,0:T(8,128)(2,1)} %kl_ref.1, bf16[256,128]{1,0:T(8,128)(2,1)} %vl_ref.1, f32[1,64]{1,0:T(1,128)} %bitcast.8, ...), custom_call_target="tpu_custom_call" | custom-call | tf_op jit(solution)/shard_map/layer/pallas_call | solution.py:798
  213.3 1.7 copy.24

commit v5 on v4

--- a/solution.py
+++ b/solution.py
@@ -36,112 +36,79 @@
 
 
 class Ring:
-    def __init__(self, buf, parts, ssem, rsem, psem, right, left, partner, last):
+    def __init__(self, buf, parts, rsem, psem, fsem, ssem, right, left, partner, last):
         self.buf, self.parts, self.last = buf, parts, last
-        self.ssem, self.rsem, self.psem = ssem, rsem, psem
+        self.rsem, self.psem, self.fsem, self.ssem = rsem, psem, fsem, ssem
         self.right, self.left, self.partner = right, left, partner
 
     def at(self, pair, side, part):
         return self.buf.at[pair, side, self.parts[part]]
 
-    def to_right(self, step, pair, part, dst_pair):
+    def copy(self, src, dst, rsem, dev):
+        return _send(src, dst, self.ssem.at[0], rsem, "sp", dev)
+
+    def begin(self, part):
+        own = self.at(0, 0, part)
+        self.copy(own, self.at(1, 0, part), self.rsem.at[1, part], self.right).start()
+        self.copy(own, self.at(1, 1, part), self.rsem.at[1, part], self.left).start()
+        self.copy(own, self.at(0, 1, part), self.psem.at[0], self.partner).start()
+
+    def got(self, ref, sem):
+        self.copy(ref, ref, sem, self.partner).wait_recv()
+
+    def pass_on(self, step, part):
+        pair, last = 2 * step - 1, self.last
+        self.got(self.buf.at[pair, pl.ds(0, 2), self.parts[part]], self.rsem.at[step, part])
+
+        @pl.when(step < last - 1)
+        def _():
+            sem = self.rsem.at[step + 1, part]
+            self.copy(self.at(pair, 0, part), self.at(pair + 2, 0, part), sem, self.right).start()
+            self.copy(self.at(pair, 1, part), self.at(pair + 2, 1, part), sem, self.left).start()
+
+        @pl.when(step == last - 1)
+        def _():
+            dev = self.right if part == 0 else self.left
+            self.copy(
+                self.at(pair, part, part), self.at(2 * last - 1, 0, part), self.fsem.at[0], dev
+            ).start()
+
+        for side in range(2):
+            self.copy(
+                self.at(pair, side, part),
+                self.at(pair + 1, side, part),
+                self.psem.at[step],
+                self.partner,
+            ).start()
+
+    def first_partner(self):
+        self.got(self.buf.at[0, 1], self.psem.at[0])
+
+    def from_partner(self, step):
+        self.got(self.buf.at[2 * step], self.psem.at[step])
+
+    def to_opposite(self):
+        pair = 2 * self.last - 1
         return _send(
-            self.at(pair, 0, part),
-            self.at(dst_pair, 0, part),
-            self.ssem.at[step, 0, part],
-            self.rsem.at[dst_pair, 0, part],
-            "sp",
-            self.right,
-        )
-
-    def to_left(self, step, pair, part, dst_pair, src_side=1, dst_side=1):
-        return _send(
-            self.at(pair, src_side, part),
-            self.at(dst_pair, dst_side, part),
-            self.ssem.at[step, 1, part],
-            self.rsem.at[dst_pair, dst_side, part],
-            "sp",
-            self.left,
-        )
-
-    def to_partner(self, pair, side, part, dst_pair, dst_side):
-        return _send(
-            self.at(pair, side, part),
-            self.at(dst_pair, dst_side, part),
-            self.psem.at[dst_pair, dst_side, part],
-            self.rsem.at[dst_pair, dst_side, part],
+            self.buf.at[pair, 0],
+            self.buf.at[pair, 1],
+            self.ssem.at[1],
+            self.fsem.at[1],
             "sp",
             self.partner,
         )
 
-    def arrived(self, pair, side, part):
-        self.to_partner(pair, side, part, pair, side).wait_recv()
-
-    def first(self, part):
-        return (
-            self.to_right(1, 0, part, 1),
-            self.to_left(1, 0, part, 1, src_side=0),
-            self.to_partner(0, 0, part, 0, 1),
-        )
-
-    def begin(self, part):
-        for copy in self.first(part):
-            copy.start()
-
-    def pass_on(self, step, part):
-        pair, last = 2 * step - 1, self.last
-        for side in range(2):
-            self.arrived(pair, side, part)
-
-        @pl.when(step < last - 1)
-        def _():
-            self.to_right(step + 1, pair, part, pair + 2).start()
-            self.to_left(step + 1, pair, part, pair + 2).start()
-
-        @pl.when(step == last - 1)
-        def _():
-            if part == 0:
-                self.to_right(step + 1, pair, 0, 2 * last - 1).start()
-            else:
-                self.to_left(step + 1, pair, 1, 2 * last - 1, dst_side=0).start()
-
-        for side in range(2):
-            self.to_partner(pair, side, part, pair + 1, side).start()
-
     def opposite(self):
-        pair = 2 * self.last - 1
-        for part in range(2):
-            self.arrived(pair, 0, part)
-            self.to_partner(pair, 0, part, pair, 1).start()
+        self.got(self.buf.at[2 * self.last - 1, 0], self.fsem.at[0])
+        self.to_opposite().start()
 
     def opposite_partner(self):
-        for part in range(2):
-            self.arrived(2 * self.last - 1, 1, part)
+        self.to_opposite().wait_recv()
 
     def finish(self):
-        last = self.last
-        for part in range(2):
-            for copy in self.first(part):
-                copy.wait_send()
-
-        def sent(step, carry):
-            pair = 2 * step - 1
-            for part in range(2):
-
-                @pl.when(step < last - 1)
-                def _():
-                    self.to_right(step + 1, pair, part, pair + 2).wait_send()
-                    self.to_left(step + 1, pair, part, pair + 2).wait_send()
-
-                for side in range(2):
-                    self.to_partner(pair, side, part, pair + 1, side).wait_send()
-            return carry
-
-        lax.fori_loop(1, last, sent, 0)
-        self.to_right(last, 2 * last - 3, 0, 2 * last - 1).wait_send()
-        self.to_left(last, 2 * last - 3, 1, 2 * last - 1, dst_side=0).wait_send()
-        for part in range(2):
-            self.to_partner(2 * last - 1, 0, part, 2 * last - 1, 1).wait_send()
+        every = self.buf.at[pl.ds(0, 2 * self.last - 1)]
+        self.copy(every, every, self.fsem.at[0], self.partner).wait_send()
+        self.to_opposite().wait_send()
 
 
 def layer_kernel(
@@ -196,13 +163,15 @@
     pick,
     lsem,
     rsem,
+    psem,
+    fsem,
     ssem,
-    psem,
     xr,
     xs,
     rsem2,
+    psem2,
+    fsem2,
     ssem2,
-    psem2,
     gr,
     gs,
     rr,
@@ -260,9 +229,10 @@
     ring = Ring(
         kvbuf,
         (pl.ds(0, tok), pl.ds(tok, kv_rows - tok)),
-        ssem,
         rsem,
         psem,
+        fsem,
+        ssem,
         right,
         left,
         partner,
@@ -271,9 +241,10 @@
     tokens = Ring(
         xbuf,
         (pl.ds(0, rows // 2), pl.ds(rows // 2, rows // 2)),
-        ssem2,
         rsem2,
         psem2,
+        fsem2,
+        ssem2,
         right,
         left,
         partner,
@@ -387,8 +358,11 @@
 
     def attend(pair):
         keys = kvbuf[pair, :, pl.ds(0, tok), :].reshape(2 * tok, tok)
+        ahead = jnp.dot(keys, qt[0], preferred_element_type=F32)
         for h, (a0, size, v0, scale) in enumerate(heads):
-            s = jnp.dot(keys, qt[h], preferred_element_type=F32)
+            s = ahead
+            if h + 1 < len(heads):
+                ahead = jnp.dot(keys, qt[h + 1], preferred_element_type=F32)
             m_old = mbuf[h]
             m_new = jnp.maximum(m_old, jnp.max(s, axis=0, keepdims=True))
             p = jnp.exp2((s - m_new) * (scale * LOG2E))
@@ -418,14 +392,11 @@
 
         @pl.when(t == 0)
         def _():
-            for part in range(2):
-                ring.arrived(0, 1, part)
+            ring.first_partner()
 
         @pl.when((phase == 0) & (t > 0))
         def _():
-            for side in range(2):
-                for part in range(2):
-                    ring.arrived(t, side, part)
+            ring.from_partner(t // 2)
 
         @pl.when(t == 2 * last - 1)
         def _():
@@ -447,31 +418,66 @@
     def project(where, owner):
         cbuf[where] = jnp.dot(hbuf[owner], wbuf[...], preferred_element_type=F32).astype(BF16)
 
-    lo, hi = pl.ds(0, rows // 2), pl.ds(rows // 2, rows // 2)
+    quarter = rows // 4
+    halves = (pl.ds(0, 2 * quarter), pl.ds(2 * quarter, 2 * quarter))
+
+    def first(part, way):
+        piece = pl.ds((2 * part + way) * quarter, quarter)
+        return _send(
+            cbuf.at[0, piece],
+            dbuf.at[3, piece],
+            xs.at[0],
+            xr.at[part, way],
+            "tp",
+            (x_right, x_left)[way],
+        )
+
+    def near(part, way):
+        return _send(
+            cbuf.at[1 + way, halves[part]],
+            dbuf.at[way, halves[part]],
+            xs.at[0],
+            xr.at[part, 2],
+            "tp",
+            (x_right, x_left)[way],
+        )
+
+    def relay(part, way):
+        piece = pl.ds((2 * part + way) * quarter, quarter)
+        return _send(
+            dbuf.at[3, piece],
+            dbuf.at[2, piece],
+            xs.at[0],
+            xr.at[part, 3],
+            "tp",
+            (x_right, x_left)[way],
+        )
+
+    def came_in(ref, sem):
+        _send(ref, ref, xs.at[0], sem, "tp", x_right).wait_recv()
+
     project(0, x_far)
-    first_r = _send(cbuf.at[0, lo], dbuf.at[3, lo], xs.at[0], xr.at[0], "tp", x_right)
-    first_l = _send(cbuf.at[0, hi], dbuf.at[3, hi], xs.at[1], xr.at[1], "tp", x_left)
-    first_r.start()
-    first_l.start()
+    for way in range(2):
+        first(0, way).start()
     project(1, x_right)
-    near_r = _send(cbuf.at[1], dbuf.at[0], xs.at[2], xr.at[2], "tp", x_right)
-    near_r.start()
+    near(0, 0).start()
     project(2, x_left)
-    near_l = _send(cbuf.at[2], dbuf.at[1], xs.at[3], xr.at[3], "tp", x_left)
-    near_l.start()
+    near(0, 1).start()
+    for way in range(2):
+        first(1, way).start()
     project(3, tp)
-    first_r.wait_recv()
-    pass_r = _send(dbuf.at[3, lo], dbuf.at[2, lo], xs.at[4], xr.at[4], "tp", x_right)
-    pass_r.start()
-    first_l.wait_recv()
-    pass_l = _send(dbuf.at[3, hi], dbuf.at[2, hi], xs.at[5], xr.at[5], "tp", x_left)
-    pass_l.start()
+    for way in range(2):
+        first(0, way).wait_recv()
+        relay(0, way).start()
+    for way in range(2):
+        near(1, way).start()
+    for way in range(2):
+        first(1, way).wait_recv()
+        relay(1, way).start()
     ring.finish()
-    near_r.wait_recv()
-    near_l.wait_recv()
-    pass_r.wait_recv()
-    pass_l.wait_recv()
-    for part, half in enumerate((lo, hi)):
+    for part, half in enumerate(halves):
+        came_in(dbuf.at[pl.ds(0, 2), half], xr.at[part, 2])
+        came_in(dbuf.at[2, half], xr.at[part, 3])
         total = (
             cbuf[3, half].astype(F32)
             + dbuf[0, half].astype(F32)
@@ -487,34 +493,36 @@
             * gain_ref[...]
         ).astype(BF16)
         tokens.begin(part)
-    for c in (first_r, first_l, near_r, near_l, pass_r, pass_l):
-        c.wait_send()
+    _send(cbuf, cbuf, xs.at[0], xr.at[0, 0], "tp", x_right).wait_send()
 
     def share_right(c):
-        return _send(gbuf.at[c, 0], gbuf.at[c, 1], gs.at[c, 0], gr.at[c, 0], "tp", x_right)
+        return _send(gbuf.at[c, 0], gbuf.at[c, 1], gs.at[0], gr.at[c, 0], "tp", x_right)
 
     def share_left(c):
-        return _send(gbuf.at[c, 0], gbuf.at[c, 2], gs.at[c, 1], gr.at[c, 1], "tp", x_left)
+        return _send(gbuf.at[c, 0], gbuf.at[c, 2], gs.at[0], gr.at[c, 0], "tp", x_left)
 
     def pass_right(c):
         return _send(
-            gbuf.at[c, 1, 0], gbuf.at[c, 3, 0], gs.at[c, 2], gr.at[c, 2], "tp", x_right
+            gbuf.at[c, 1, 0], gbuf.at[c, 3, 0], gs.at[0], gr.at[c, 1], "tp", x_right
         )
 
     def pass_left(c):
-        return _send(gbuf.at[c, 2, 1], gbuf.at[c, 3, 1], gs.at[c, 3], gr.at[c, 3], "tp", x_left)
+        return _send(gbuf.at[c, 2, 1], gbuf.at[c, 3, 1], gs.at[0], gr.at[c, 1], "tp", x_left)
 
     def far_right(c):
-        return _send(pbuf.at[c, 3, 0], rbuf.at[c, 0], rs.at[c, 0], rr.at[c, 0], "tp", x_right)
+        return _send(pbuf.at[c, 3, 0], rbuf.at[c, 0], rs.at[0], rr.at[c, 0], "tp", x_right)
 
     def far_left(c):
-        return _send(pbuf.at[c, 3, 1], rbuf.at[c, 1], rs.at[c, 1], rr.at[c, 1], "tp", x_left)
+        return _send(pbuf.at[c, 3, 1], rbuf.at[c, 1], rs.at[0], rr.at[c, 0], "tp", x_left)
 
     def near_right(c):
-        return _send(pbuf.at[c, 2], fbuf.at[c, 0], rs.at[c, 2], rr.at[c, 2], "tp", x_right)
+        return _send(pbuf.at[c, 2], fbuf.at[c, 0], rs.at[0], rr.at[c, 1], "tp", x_right)
 
     def near_left(c):
-        return _send(pbuf.at[c, 1], fbuf.at[c, 1], rs.at[c, 3], rr.at[c, 3], "tp", x_left)
+        return _send(pbuf.at[c, 1], fbuf.at[c, 1], rs.at[0], rr.at[c, 1], "tp", x_left)
+
+    def both(ref, sem):
+        _send(ref, ref, gs.at[0], sem, "tp", x_right).wait_recv()
 
     def seats_of(c):
         row = _iota((16, tok), 0)
@@ -558,14 +566,11 @@
 
         @pl.when(c == 0)
         def _():
-            for part in range(2):
-                tokens.arrived(0, 1, part)
+            tokens.first_partner()
 
         @pl.when((c > 0) & (c < last))
         def _():
-            for side in range(2):
-                for part in range(2):
-                    tokens.arrived(2 * c, side, part)
+            tokens.from_partner(c)
 
         @pl.when(step == last)
         def _():
@@ -581,9 +586,8 @@
 
         @pl.when((c >= 1) & (c < last + 1))
         def _():
-            share_right(c - 1).wait_recv()
+            both(gbuf.at[c - 1, pl.ds(1, 2)], gr.at[c - 1, 0])
             pass_right(c - 1).start()
-            share_left(c - 1).wait_recv()
             pass_left(c - 1).start()
 
         @pl.when(c == 2)
@@ -593,8 +597,7 @@
 
         @pl.when((c >= 2) & (c < last + 2))
         def _():
-            pass_right(c - 2).wait_recv()
-            pass_left(c - 2).wait_recv()
+            both(gbuf.at[c - 2, 3], gr.at[c - 2, 1])
             run_experts(c - 2)
 
     def home(c, q):
@@ -609,7 +612,7 @@
     def give(c, q):
         dev, pair, side = home(c, q)
         return _send(
-            obuf.at[c, q], ret.at[pair, side], ts.at[c, q], tr.at[pair, side], "sp", dev
+            obuf.at[c, q], ret.at[pair, side], ts.at[min(q, 1)], tr.at[1], "sp", dev
         )
 
     def give_last():
@@ -617,25 +620,29 @@
         return _send(
             obuf.at[last - 1, 3],
             ret.at[2 * last - 1, 1],
-            ts.at[last - 1, 3],
-            tr.at[2 * last - 1, 1],
+            ts.at[1],
+            tr.at[1],
             "sp",
             dev,
         )
 
+    start = last // 2 - 1
+
     def order(i):
-        half = last // 2
-        late = i // half
-        return (1 - late) * (i + half) + late * (last - 1 - i)
+        high = last - start
+        late = i // high
+        return (1 - late) * (i + start) + late * (last - 1 - i)
+
+    def give_partner():
+        return _send(obuf.at[0, 1], ret.at[0, 1], ts.at[1], tr.at[0], "sp", partner)
 
     def return_turn(i):
         @pl.when((i >= 1) & (i < last + 1))
         def _():
             c = order(i - 1)
-            far_right(c).wait_recv()
+            both(rbuf.at[c], rr.at[c, 0])
             pbuf[c, 2, 0] = (pbuf[c, 2, 0].astype(F32) + rbuf[c, 0].astype(F32)).astype(BF16)
             near_right(c).start()
-            far_left(c).wait_recv()
             pbuf[c, 1, 1] = (pbuf[c, 1, 1].astype(F32) + rbuf[c, 1].astype(F32)).astype(BF16)
             near_left(c).start()
 
@@ -648,8 +655,7 @@
         @pl.when(i >= 2)
         def _():
             c = order(i - 2)
-            near_right(c).wait_recv()
-            near_left(c).wait_recv()
+            both(fbuf.at[c], rr.at[c, 1])
             total = pbuf[c, 0].astype(F32) + fbuf[c, 0].astype(F32) + fbuf[c, 1].astype(F32)
             total = total.astype(BF16).reshape(32, width)
             split = jnp.concatenate([total[:, : width // 2], total[:, width // 2 :]], axis=0)
@@ -659,12 +665,13 @@
             @pl.when(c > 0)
             def _():
                 give(c, 0).start()
+                give(c, 1).start()
 
             @pl.when(c == 0)
             def _():
                 ret[0, 0] = obuf[0, 0]
-
-            give(c, 1).start()
+                give_partner().start()
+
             give(c, 2).start()
 
             @pl.when(c < last - 1)
@@ -677,32 +684,20 @@
 
     def turn(t, carry):
         gather_turn(t)
-        return_turn(t - (last - 1))
+        return_turn(t - (start + 2))
         return carry
 
-    lax.fori_loop(0, 2 * last + 1, turn, 0)
+    lax.fori_loop(0, last + start + 4, turn, 0)
 
     tokens.finish()
 
-    def left_all(c, carry):
-        for copy in (share_right, share_left, pass_right, pass_left):
-            copy(c).wait_send()
-        for copy in (far_right, far_left, near_right, near_left):
-            copy(c).wait_send()
-        return carry
-
-    lax.fori_loop(0, last, left_all, 0)
-
-    def came(c, carry):
-        @pl.when(c > 0)
-        def _():
-            give(c, 0).wait_recv()
-
-        for q in (1, 2, 3):
-            give(c, q).wait_recv()
-        return carry
-
-    lax.fori_loop(0, last, came, 0)
+    sent = gbuf.at[pl.ds(0, 3 * (last // 4))]
+    _send(sent, sent, gs.at[0], gr.at[0, 0], "tp", x_right).wait_send()
+    sent = pbuf.at[pl.ds(0, 3 * (last // 4))]
+    _send(sent, sent, rs.at[0], rr.at[0, 0], "tp", x_right).wait_send()
+    home_all = ret.at[pl.ds(1, 2 * last - 1)]
+    give_partner().wait_recv()
+    _send(home_all, home_all, ts.at[0], tr.at[1], "sp", partner).wait_recv()
 
     back = ret[...].reshape(ret.shape[0] * 32, width // 2)
     picked = jnp.dot(pick[...], back, preferred_element_type=F32)
@@ -715,16 +710,10 @@
     out_ref[:, : width // 2] = (out[:, : width // 2] + lower).astype(BF16)
     out_ref[:, width // 2 :] = (out[:, width // 2 :] + upper).astype(BF16)
 
-    def gone(c, carry):
-        @pl.when(c > 0)
-        def _():
-            give(c, 0).wait_send()
-
-        for q in (1, 2, 3):
-            give(c, q).wait_send()
-        return carry
-
-    lax.fori_loop(0, last, gone, 0)
+    sent = obuf.at[pl.ds(1, last - 1), 0]
+    _send(sent, sent, ts.at[0], tr.at[1], "sp", partner).wait_send()
+    sent = obuf.at[pl.ds(0, 3 * (last // 4))]
+    _send(sent, sent, ts.at[1], tr.at[1], "sp", partner).wait_send()
 
 
 def turn_tables(places, size, by_row):
@@ -828,20 +817,22 @@
             V((64, 64), BF16),
             V((4 * rows, pairs * 32), BF16),
             dma((7,)),
-            dma((pairs, 2, 2)),
-            dma((chunks + 1, 2, 2)),
-            dma((pairs, 2, 2)),
-            dma((6,)),
-            dma((6,)),
-            dma((pairs, 2, 2)),
-            dma((chunks + 1, 2, 2)),
-            dma((pairs, 2, 2)),
-            dma((chunks, 4)),
-            dma((chunks, 4)),
-            dma((chunks, 4)),
-            dma((chunks, 4)),
-            dma((pairs, 2)),
-            dma((chunks, 4)),
+            dma((chunks, 2)),
+            dma((chunks,)),
+            dma((2,)),
+            dma((2,)),
+            dma((2, 4)),
+            dma((1,)),
+            dma((chunks, 2)),
+            dma((chunks,)),
+            dma((2,)),
+            dma((2,)),
+            dma((chunks, 2)),
+            dma((1,)),
+            dma((chunks, 2)),
+            dma((1,)),
+            dma((2,)),
+            dma((2,)),
         ],
         compiler_params=pltpu.CompilerParams(
             collective_id=0, has_side_effects=True, vmem_limit_bytes=58 * 1024 * 1024

time: 215 us -> 198 us (0.921)
  Pallas kernels: 212 us -> 195 us
    pallas_call x1, Pallas kernels: 212 us -> 195 us  [on_device(): pl.pallas_call(functools.partial(layer_kernel, tuple(heads)), out_shape=j...]
where the time goes in v5:
time: 198 us
  Pallas kernels  195 us (98%)
  local copies, waits for them, and re-layouts  3.05 us (2%)
    pallas_call x1, Pallas kernels, on_device(): pl.pallas_call(functools.partial(layer_kernel, tuple(heads)), out_shape=j...  195 us

profile of v5, /device:TPU:33, one launch (start us, length us, event | category | flops | bytes accessed | tf_op | source)
XLA Modules:
  0.0 197.9 jit_solution(9452395520777703592)
XLA Ops:
  0.0 1.4 copy.22.score_ref
  1.4 194.9 %layer.1 = bf16[64,2048]{1,0:T(8,128)(2,1)} custom-call(bf16[256,256]{1,0:T(8,128)(2,1)} %qs_ref.1, bf16[256,128]{1,0:T(8,128)(2,1)} %ks_ref.1, bf16[256,128]{1,0:T(8,128)(2,1)} %vs_ref.1, bf16[256,256]{1,0:T(8,128)(2,1)} %ql_ref.1, bf16[256,128]{1,0:T(8,128)(2,1)} %kl_ref.1, bf16[256,128]{1,0:T(8,128)(2,1)} %vl_ref.1, f32[1,64]{1,0:T(1,128)} %bitcast.8, ...), custom_call_target="tpu_custom_call" | custom-call | tf_op jit(solution)/shard_map/layer/pallas_call | solution.py:787
  196.3 1.7 copy.24

commit v6 on v5

--- a/solution.py
+++ b/solution.py
@@ -637,6 +637,12 @@
         return _send(obuf.at[0, 1], ret.at[0, 1], ts.at[1], tr.at[0], "sp", partner)
 
     def return_turn(i):
+        @pl.when((i >= 0) & (i < last))
+        def _():
+            c = order(i)
+            far_right(c).start()
+            far_left(c).start()
+
         @pl.when((i >= 1) & (i < last + 1))
         def _():
             c = order(i - 1)
@@ -645,12 +651,6 @@
             near_right(c).start()
             pbuf[c, 1, 1] = (pbuf[c, 1, 1].astype(F32) + rbuf[c, 1].astype(F32)).astype(BF16)
             near_left(c).start()
-
-        @pl.when((i >= 0) & (i < last))
-        def _():
-            c = order(i)
-            far_right(c).start()
-            far_left(c).start()
 
         @pl.when(i >= 2)
         def _():
@@ -702,8 +702,10 @@
     back = ret[...].reshape(ret.shape[0] * 32, width // 2)
     picked = jnp.dot(pick[...], back, preferred_element_type=F32)
     scores = score_ref[...]
-    scores = scores / (scores[:, 0:1] + scores[:, 1:2])
-    one, two = scores[:, 0:1], scores[:, 1:2]
+    scores = scores / (scores[0:1, :] + scores[1:2, :])
+    on_row = _iota((rows, rows), 0) == _iota((rows, rows), 1)
+    one = jnp.sum(jnp.where(on_row, scores[0:1, :], 0.0), axis=1, keepdims=True)
+    two = jnp.sum(jnp.where(on_row, scores[1:2, :], 0.0), axis=1, keepdims=True)
     out = abuf[...].astype(F32)
     lower = picked[:rows] * one + picked[rows : 2 * rows] * two
     upper = picked[2 * rows : 3 * rows] * one + picked[3 * rows :] * two
@@ -856,7 +858,7 @@
         residual_in,
         norm_gain.reshape(1, -1),
         routes.T,
-        route_scores,
+        route_scores.T,
         expert_gate,
         expert_up,
         expert_down,

time: 198 us -> 197 us (level)
  no operation moved by 1% of the time
where the time goes in v6:
time: 197 us
  Pallas kernels  195 us (99%)
    pallas_call x1, Pallas kernels, on_device(): pl.pallas_call(functools.partial(layer_kernel, tuple(heads)), out_shape=j...  195 us

profile of v6, /device:TPU:33, one launch (start us, length us, event | category | flops | bytes accessed | tf_op | source)
XLA Modules:
  0.0 196.7 jit_solution(2419516541312700732)
XLA Ops:
  0.0 195.0 %layer.1 = bf16[64,2048]{1,0:T(8,128)(2,1)} custom-call(bf16[256,256]{1,0:T(8,128)(2,1)} %qs_ref.1, bf16[256,128]{1,0:T(8,128)(2,1)} %ks_ref.1, bf16[256,128]{1,0:T(8,128)(2,1)} %vs_ref.1, bf16[256,256]{1,0:T(8,128)(2,1)} %ql_ref.1, bf16[256,128]{1,0:T(8,128)(2,1)} %kl_ref.1, bf16[256,128]{1,0:T(8,128)(2,1)} %vl_ref.1, f32[1,64]{1,0:T(1,128)} %bitcast.10, ...), custom_call_target="tpu_custom_call" | custom-call | tf_op jit(solution)/shard_map/layer/pallas_call | solution.py:789
  195.0 1.7 copy.23
